TPU v7x, 32 devices: a whole 2x2x4 slice. The times are simulated.
32 devices in a mesh: sp: 8 (over z, y), tp: 4 (over x, core).
Axes of the slice: x: 2, y: 2, z: 4, core: 2. Of those that a mesh axis runs over, the one named last changes fastest.
Arguments:
- stream: bfloat16 [1536, 2048], P('sp'), may hold values from -6 to 6
- upstream: bfloat16 [1536, 2048], P('sp'), may hold values from -6 to 6
- expert_gain: float32 [2048], replicated, may hold values from 0.1 to 1.9
- expert_ids: int32 [1536, 2], P('sp'), may hold values from 0 to 7, all different within a row; in each aligned block of 192 rows (0 to 191, 192 to 383, ...) at most 60 rows name the same one
- group_weight: float32 [1536], P('sp'), may hold values from 0.25 to 1
- pair_scores: float32 [1536, 2], P('sp'), may hold values from -6 to 6
- gate_weight: bfloat16 [8, 2048, 1024], P('sp', None, 'tp'), may hold values from -0.125 to 0.125
- up_weight: bfloat16 [8, 2048, 1024], P('sp', None, 'tp'), may hold values from -0.125 to 0.125
- down_weight: bfloat16 [8, 1024, 2048], P('sp', 'tp'), may hold values from -0.1875 to 0.1875
- mixer_weight: bfloat16 [1024, 2048], P('tp'), may hold values from -0.1875 to 0.1875
- filtered: bfloat16 [1536, 1024], P('sp', 'tp'), may hold values from -1000 to 1000
- channel_gain: float32 [1024], P('tp'), may hold values from 0.1 to 1.9
- kernel_taps: float32 [31, 1024], P(None, 'tp'), may hold values from -1 to 1
- value_branch: bfloat16 [1536, 1024], P('sp', 'tp'), may hold values from -6 to 6
- gate_branch: bfloat16 [1536, 1024], P('sp', 'tp'), may hold values from -6 to 6
Outputs:
- gradient_value: bfloat16 [1536, 1024], P('sp', 'tp')
- gradient_gating: bfloat16 [1536, 1024], P('sp', 'tp')
- gradient_mixer: float32 [2048, 1024], P('sp', 'tp')
- gradient_gate: float32 [8, 2048, 1024], P('sp', None, 'tp')
- gradient_up: float32 [8, 2048, 1024], P('sp', None, 'tp')
- gradient_down: float32 [8, 1024, 2048], P('sp', 'tp')
Inputs may be any that keep to these rules, and one draw needn't show every extreme that they name: `expert_ids`: the two experts of a token differ. Among the rows of one index of sp, at most 60 routes name the same expert, and in every draw some expert is named by exactly 60 of them.
All inputs are finite; a program needn't handle non-finite values.
Results may differ from a plain program's by a relative error of at most 0.012.
Values may be sent and summed in bfloat16 or wider, within the bound.
A program may use at most 64 MiB of HBM per device.

v0:
```python
import functools

import jax
import jax.numpy as jnp
from jax import lax
from jax.experimental import pallas as pl
from jax.experimental.pallas import tpu as pltpu
from jax.sharding import PartitionSpec as P

EPS = 1e-06
MESH = pl.DeviceIdType.MESH
F32 = jnp.float32
BF16 = jnp.bfloat16
HIGHEST = lax.Precision.HIGHEST


def silu_slope(value, sigma):
    return sigma * (1.0 + value * (1.0 - sigma))


def contract_last(left, right, precision=None):
    return lax.dot_general(
        left, right, (((1,), (1,)), ((), ())), preferred_element_type=F32, precision=precision
    )


def contract_first(left, right):
    return lax.dot_general(left, right, (((0,), (0,)), ((), ())), preferred_element_type=F32)


def round_up(value, unit):
    return -(-value // unit) * unit


def flip(index, mask):
    bit = 1
    while bit <= mask:
        if mask & bit:
            index = index + bit - 2 * bit * ((index // bit) % 2)
        bit *= 2
    return index


def low_bit(mask):
    return mask & -mask


def bits_below(limit):
    found, bit = [], 1
    while bit < limit:
        found.append(bit)
        bit *= 2
    return found[::-1]


def remote(src, dst, send, recv, where):
    return pltpu.make_async_remote_copy(
        src_ref=src, dst_ref=dst, send_sem=send, recv_sem=recv, device_id=where, device_id_type=MESH
    )


def enter(me, n, tp, groups):
    barrier = pltpu.get_barrier_semaphore()

    def greet(i, carry):
        pl.semaphore_signal(
            barrier, inc=1, device_id={"sp": lax.rem(me + i, n)}, device_id_type=MESH
        )
        return carry

    lax.fori_loop(1, n, greet, 0)
    for bit in bits_below(groups):
        pl.semaphore_signal(barrier, inc=1, device_id={"tp": flip(tp, bit)}, device_id_type=MESH)
    pl.semaphore_wait(barrier, n - 1 + len(bits_below(groups)))


class Spread:
    def __init__(self, place, tp, groups, send, recv):
        self.place, self.tp, self.groups = place, tp, groups
        self.send_sem, self.recv_sem = send, recv

    def copy(self, mask, bit):
        ref = self.place(flip(self.tp, mask))
        return remote(
            ref,
            ref,
            self.send_sem(mask | bit),
            self.recv_sem(mask | bit),
            {"tp": flip(self.tp, bit)},
        )

    def wait(self, mask):
        ref = self.place(flip(self.tp, mask))
        where = {"tp": flip(self.tp, low_bit(mask))}
        remote(ref, ref, self.send_sem(mask), self.recv_sem(mask), where).wait_recv()

    def begin(self):
        for bit in bits_below(self.groups):
            self.copy(0, bit).start()

    def masks(self):
        return sorted(range(1, self.groups), key=lambda m: (bin(m).count("1"), -low_bit(m)))

    def relay(self):
        for mask in self.masks():
            onward = bits_below(low_bit(mask))
            if onward:
                self.wait(mask)
                for bit in onward:
                    self.copy(mask, bit).start()

    def finish(self):
        for mask in self.masks():
            if not bits_below(low_bit(mask)):
                self.wait(mask)
        for mask in range(1, self.groups):
            self.copy(mask - low_bit(mask), low_bit(mask)).wait_send()


def each(first, last, step):
    def run(i, carry):
        step(i)
        return carry

    lax.fori_loop(first, last, run, 0)


def dispatch_kernel(
    n,
    groups,
    pcap,
    stream,
    upstream,
    gain,
    ids,
    weight,
    scores,
    filtered,
    rows,
    cots,
    places,
    stats,
    send_rows,
    send_cots,
    sp_send,
    sp_recv,
    tp_send,
    tp_recv,
    st_send,
    st_recv,
):
    me, tp = lax.axis_index("sp"), lax.axis_index("tp")
    tokens, width = stream.shape
    column = width // groups
    enter(me, n, tp, groups)

    filt = filtered[...]
    square = filt.astype(F32) * filt.astype(F32)
    high = square.astype(BF16)
    low = (square - high.astype(F32)).astype(BF16)
    ones = jnp.ones((8, filt.shape[1]), BF16)
    total = contract_last(ones, filt)
    total_square = contract_last(ones, high) + contract_last(ones, low)
    line = lax.broadcasted_iota(jnp.int32, total.shape, 0)
    stats[tp] = jnp.where(line == 0, total, total_square)
    sums = Spread(
        lambda o: stats.at[o], tp, groups, lambda m: st_send.at[m], lambda m: st_recv.at[m]
    )
    sums.begin()

    routes = 2 * tokens
    onehot = (lax.broadcasted_iota(jnp.int32, (n, routes), 0) == ids[...]).astype(F32)
    earlier = (
        lax.broadcasted_iota(jnp.int32, (routes, routes), 0)
        < lax.broadcasted_iota(jnp.int32, (routes, routes), 1)
    ).astype(F32).astype(BF16)
    before = jnp.dot(onehot.astype(BF16), earlier, preferred_element_type=F32)
    base = (lax.broadcasted_iota(jnp.int32, (n, routes), 0) * pcap).astype(F32)
    slot = jnp.sum(onehot * (before + base), axis=0, keepdims=True).astype(jnp.int32)
    slot_at = lax.broadcasted_iota(jnp.int32, (n * pcap, tokens), 0)
    first = (slot_at == slot[:, :tokens]).astype(F32).astype(BF16)
    second = (slot_at == slot[:, tokens:]).astype(F32).astype(BF16)
    both = first + second
    places[...] = both

    stream_f = stream[...].astype(F32)
    inv_rms = lax.rsqrt(jnp.mean(stream_f * stream_f, axis=1, keepdims=True) + EPS)
    cols = pl.ds(pl.multiple_of(tp * column, column), column)
    normed = (stream[:, cols].astype(F32) * inv_rms * gain[:, cols]).astype(BF16)
    send_rows[...] = jnp.dot(both, normed, preferred_element_type=F32).astype(BF16)
    spread = scores[:, 0:1] - scores[:, 1:2]
    up = upstream[:, cols].astype(F32)
    scaled_a = (weight[...] * jax.nn.sigmoid(spread) * up).astype(BF16)
    scaled_b = (weight[...] * jax.nn.sigmoid(-spread) * up).astype(BF16)
    send_cots[...] = (
        jnp.dot(first, scaled_a, preferred_element_type=F32)
        + jnp.dot(second, scaled_b, preferred_element_type=F32)
    ).astype(BF16)

    pairs = ((send_rows, rows), (send_cots, cots))

    def block(j):
        return pl.ds(pl.multiple_of(j * pcap, pcap), pcap)

    def place(full, s, o):
        return full.at[block(s), pl.ds(pl.multiple_of(o * column, column), column)]

    def sp_copy(a, i, j, s):
        src, full = pairs[a]
        return remote(
            src.at[block(j)], place(full, s, tp), sp_send.at[a, i], sp_recv.at[a, i], {"sp": j}
        )

    def send(i):
        for a in range(2):
            sp_copy(a, i, lax.rem(me + i, n), me).start()

    window = min(n - 1, 3)
    each(1, window + 1, send)
    for src, full in pairs:
        full[block(me), cols] = src[block(me)]

    def gather(a, i):
        s = lax.rem(me + n - i, n)
        return Spread(
            lambda o: place(pairs[a][1], s, o),
            tp,
            groups,
            lambda m: tp_send.at[a, i, m],
            lambda m: tp_recv.at[a, i, m],
        )

    def arrive(i):
        for a in range(2):
            s = lax.rem(me + n - i, n)
            sp_copy(a, i, s, s).wait_recv()
            if a == 0:
                pl.when(i + window < n)(lambda: send(i + window))
            gather(a, i).begin()
            gather(a, i - 1).relay()

    for a in range(2):
        gather(a, 0).begin()
    each(1, n, arrive)
    for a in range(2):
        gather(a, n - 1).relay()
    sums.relay()
    sums.finish()

    def close(i):
        for a in range(2):
            gather(a, i).finish()

    each(0, n, close)

    def sent(i):
        for a in range(2):
            sp_copy(a, i, lax.rem(me + i, n), me).wait_send()

    each(1, n, sent)


def tail_kernel(
    n,
    groups,
    pcap,
    partial,
    places,
    stats,
    stream,
    upstream,
    gain,
    mixer,
    filtered,
    channel_gain,
    taps,
    value,
    gate,
    out_value,
    out_gating,
    out_mixer,
    halves,
    passing,
    keep,
    crossed,
    outgoing,
    back,
    grad_normed,
    grad_stream,
    staged,
    grad_all,
    act_all,
    slopes,
    halo_out,
    halo_in,
    ext,
    core_send,
    core_recv,
    x_send,
    x_recv,
    sp_send,
    sp_recv,
    gn_send,
    gn_recv,
    far_send,
    far_recv,
    near_send,
    near_recv,
    gs_send,
    gs_recv,
    ga_send,
    ga_recv,
    sl_send,
    sl_recv,
    halo_send,
    halo_recv,
):
    me, tp = lax.axis_index("sp"), lax.axis_index("tp")
    tokens, width = stream.shape
    column = width // groups
    channels = filtered.shape[1] * groups
    portion = tokens // groups
    db = width // n
    pdb = grad_all.shape[1]
    reach = taps.shape[0] - 1
    hpad = halo_in.shape[0]
    enter(me, n, tp, groups)

    def block(j):
        return pl.ds(pl.multiple_of(j * pcap, pcap), pcap)

    def quarter(q):
        return pl.ds(pl.multiple_of(q * column, column), column)

    mate = flip(tp, 1)
    half = groups // 2

    def chunk(i):
        return lax.rem(me + 1 + i, n)

    def core_copy(i, h):
        j = chunk(i)
        return remote(
            partial.at[block(j), quarter(lax.rem(mate, 2) + 2 * h)],
            halves.at[block(j), pl.ds(h * column, column)],
            core_send.at[i, h],
            core_recv.at[i, h],
            {"tp": mate},
        )

    def start_core(i):
        for h in range(half):
            core_copy(i, h).start()

    each(0, n, start_core)

    sums = stats[0]
    for o in range(1, groups):
        sums = sums + stats[o]
    eye = (
        lax.broadcasted_iota(jnp.int32, (tokens, tokens), 0)
        == lax.broadcasted_iota(jnp.int32, (tokens, tokens), 1)
    ).astype(F32)
    sums = contract_last(eye, sums, HIGHEST)
    mean_c = sums[:, 0:1] / channels
    variance = sums[:, 1:2] / channels - mean_c * mean_c
    inv_std = lax.rsqrt(variance + EPS)
    centred = (filtered[...].astype(F32) - mean_c) * inv_std
    normal_out = centred * channel_gain[...]
    sig_norm = jax.nn.sigmoid(normal_out)

    def act_rows(s):
        return pl.ds(pl.multiple_of(s * tokens, tokens), tokens)

    act_all[act_rows(me)] = (normal_out * sig_norm).astype(BF16)
    buddy = flip(me, 1)

    def far_copy(i, to, origin):
        ref = act_all.at[act_rows(origin)]
        return remote(ref, ref, far_send.at[i], far_recv.at[i], {"sp": to})

    def near_copy(i, holder):
        ref = act_all.at[act_rows(lax.rem(holder + n - 2 * i, n))]
        return remote(ref, ref, near_send.at[i], near_recv.at[i], {"sp": buddy})

    each(1, n // 2, lambda i: far_copy(i, lax.rem(me + 2 * i, n), me).start())
    near_copy(0, me).start()

    def x_copy(i, h):
        j = chunk(i)
        peer = lax.rem(tp, 2) + 2 * h
        ref = passing.at[block(j), pl.ds(h * column, column)]
        return peer, ref

    bits = [bit // 2 for bit in bits_below(groups) if bit > 1]
    mine = tp // 2

    def cross(i, m, wait):
        j = chunk(i)
        h = flip(mine, m)
        return remote(
            passing.at[block(j), pl.ds(pl.multiple_of(h * column, column), column)],
            crossed.at[block(j), pl.ds((m - 1) * column, column)],
            x_send.at[i, m],
            x_recv.at[i, m],
            {"tp": flip(tp, 2 * m)},
        )

    def add_core(i):
        j = chunk(i)
        for h in range(half):
            core_copy(i, h).wait_recv()
        for h in range(half):
            own = partial[block(j), quarter(lax.rem(tp, 2) + 2 * h)].astype(F32)
            passing[block(j), pl.ds(h * column, column)] = (
                own + halves[block(j), pl.ds(h * column, column)].astype(F32)
            ).astype(BF16)
        for m in range(1, half):
            cross(i, m, False).start()

    def home_copy(i, s):
        return remote(
            outgoing.at[block(chunk(i))],
            back.at[block(s)],
            sp_send.at[i],
            sp_recv.at[i],
            {"sp": chunk(i)},
        )

    def total_of(i):
        j = chunk(i)
        for m in range(1, half):
            cross(i, m, True).wait_recv()
        total = passing[block(j), pl.ds(pl.multiple_of(mine * column, column), column)].astype(F32)
        for m in range(1, half):
            total = total + crossed[block(j), pl.ds((m - 1) * column, column)].astype(F32)
        return total.astype(BF16)

    def add_x(i):
        outgoing[block(chunk(i))] = total_of(i)
        home_copy(i, me).start()

    add_core(0)

    def both(i):
        add_core(i)
        add_x(i - 1)

    each(1, n, both)
    back[block(me)] = total_of(n - 1)

    def relay_act(i):
        origin = lax.rem(me + n - 2 * i, n)
        far_copy(i, origin, origin).wait_recv()
        near_copy(i, me).start()

    each(1, n // 2, relay_act)

    inv_rms = jnp.zeros((tokens, 1), F32)
    for q in range(groups):
        piece = stream[:, q * column : (q + 1) * column].astype(F32)
        inv_rms = inv_rms + jnp.sum(piece * piece, axis=1, keepdims=True)
    inv_rms = lax.rsqrt(inv_rms / width + EPS)

    def came_home(i):
        s = lax.rem(me + n - 1 - i, n)
        home_copy(i, s).wait_recv()

    each(0, n - 1, came_home)
    grad_normed[:, quarter(tp)] = contract_first(places[...], back[...]).astype(BF16)
    gather = Spread(
        lambda o: grad_normed.at[:, quarter(o)],
        tp,
        groups,
        lambda m: gn_send.at[m],
        lambda m: gn_recv.at[m],
    )
    gather.begin()
    gather.relay()
    gather.finish()

    inner = jnp.zeros((tokens, 1), F32)
    for q in range(groups):
        at = slice(q * column, (q + 1) * column)
        weighted = grad_normed[:, at].astype(F32) * gain[:, at]
        inner = inner + jnp.sum(weighted * stream[:, at].astype(F32), axis=1, keepdims=True)
    inner = inv_rms * inv_rms * inv_rms * (inner / width)
    for q in range(groups):
        at = slice(q * column, (q + 1) * column)
        weighted = grad_normed[:, at].astype(F32) * gain[:, at]
        grad_stream[:, at] = (
            upstream[:, at].astype(F32) + inv_rms * weighted - stream[:, at].astype(F32) * inner
        ).astype(BF16)

    def part(s, o):
        start = pl.multiple_of(s * tokens + o * portion, portion)
        return grad_all.at[pl.ds(start, portion)]

    my_rows = pl.ds(pl.multiple_of(tp * portion, portion), portion)
    if db == pdb:

        def cut(j):
            return grad_stream.at[my_rows, pl.ds(pl.multiple_of(j * db, db), db)]

        grad_all[act_rows(me)] = grad_stream[:, pl.ds(pl.multiple_of(me * db, db), db)]
    else:

        def pick(j):
            where = lax.broadcasted_iota(jnp.int32, (width, pdb), 0)
            lane = lax.broadcasted_iota(jnp.int32, (width, pdb), 1)
            return ((where == lane + j * db) & (lane < db)).astype(F32).astype(BF16)

        def stage(j):
            staged[j] = jnp.dot(
                grad_stream[my_rows], pick(j), preferred_element_type=F32
            ).astype(BF16)

        each(0, n, stage)

        def cut(j):
            return staged.at[j]

        grad_all[act_rows(me)] = jnp.dot(
            grad_stream[...], pick(me), preferred_element_type=F32
        ).astype(BF16)

    def cut_copy(i, j, s):
        return remote(cut(j), part(s, tp), gs_send.at[i], gs_recv.at[i], {"sp": j})

    each(1, n, lambda i: cut_copy(i, lax.rem(me + i, n), me).start())

    grad_act = contract_last(grad_stream[...], mixer[...])
    grad_centred = grad_act * silu_slope(normal_out, sig_norm) * channel_gain[...]
    ones = jnp.ones((8, filtered.shape[1]), F32)
    slope_sum = contract_last(ones, grad_centred, HIGHEST)
    slope_cross = contract_last(ones, grad_centred * centred, HIGHEST)
    line = lax.broadcasted_iota(jnp.int32, slope_sum.shape, 0)
    slopes[tp] = jnp.where(line == 0, slope_sum, slope_cross)
    meet = Spread(
        lambda o: slopes.at[o], tp, groups, lambda m: sl_send.at[m], lambda m: sl_recv.at[m]
    )
    meet.begin()
    meet.relay()
    meet.finish()
    sums = slopes[0]
    for o in range(1, groups):
        sums = sums + slopes[o]
    sums = contract_last(eye, sums, HIGHEST)
    grad_filtered = (
        inv_std
        * (grad_centred - sums[:, 0:1] / channels - centred * (sums[:, 1:2] / channels))
    ).astype(BF16)
    halo_out[...] = grad_filtered[:hpad]
    ext[:tokens] = grad_filtered.astype(F32)

    def halo_copy():
        return remote(halo_out, halo_in, halo_send, halo_recv, {"sp": lax.rem(me + n - 1, n)})

    halo_copy().start()

    def spread_cut(i):
        s = lax.rem(me + n - i, n)
        return Spread(
            lambda o: part(s, o),
            tp,
            groups,
            lambda m: ga_send.at[i, m],
            lambda m: ga_recv.at[i, m],
        )

    def cut_arrives(i):
        s = lax.rem(me + n - i, n)
        cut_copy(i, s, s).wait_recv()
        spread_cut(i).begin()

    each(1, n, cut_arrives)

    halo_copy().wait_recv()
    inside = jnp.where(me < n - 1, 1.0, 0.0)
    ext[tokens:] = halo_in[...].astype(F32) * inside
    each(1, n, lambda i: spread_cut(i).relay())
    mixed = jnp.zeros((tokens, filtered.shape[1]), F32)
    for k in range(reach + 1):
        mixed = mixed + taps[k : k + 1] * ext[reach - k : reach - k + tokens]
    sig_gate = jax.nn.sigmoid(gate[...].astype(F32))
    out_value[...] = (mixed * sig_gate).astype(BF16)
    out_gating[...] = (mixed * value[...].astype(F32) * sig_gate * (1.0 - sig_gate)).astype(BF16)

    each(1, n, lambda i: spread_cut(i).finish())
    each(0, n // 2, lambda i: near_copy(i, buddy).wait_recv())
    out_mixer[...] = contract_first(grad_all[...], act_all[...])[:db]

    halo_copy().wait_send()
    each(1, n, lambda i: cut_copy(i, lax.rem(me + i, n), me).wait_send())
    each(1, n // 2, lambda i: far_copy(i, lax.rem(me + 2 * i, n), me).wait_send())
    each(0, n // 2, lambda i: near_copy(i, me).wait_send())
    each(0, n - 1, lambda i: home_copy(i, me).wait_send())

    def sums_sent(i):
        for h in range(half):
            core_copy(i, h).wait_send()
        for m in range(1, half):
            cross(i, m, True).wait_send()

    each(0, n, sums_sent)


def call(kernel, collective_id, outs, scratch, args):
    return pl.pallas_call(
        kernel,
        out_shape=outs,
        in_specs=[pl.BlockSpec(memory_space=pltpu.VMEM)] * len(args),
        out_specs=[pl.BlockSpec(memory_space=pltpu.VMEM)] * len(outs),
        scratch_shapes=scratch,
        compiler_params=pltpu.CompilerParams(
            collective_id=collective_id, has_side_effects=True, vmem_limit_bytes=40 << 20
        ),
    )(*args)


def body(
    stream,
    upstream,
    expert_gain,
    expert_ids,
    group_weight,
    pair_scores,
    gate_weight,
    up_weight,
    down_weight,
    mixer_weight,
    filtered,
    channel_gain,
    kernel_taps,
    value_branch,
    gate_branch,
):
    n, groups = lax.axis_size("sp"), lax.axis_size("tp")
    tokens, width = stream.shape
    capacity = max(2, 5 * tokens // (2 * n))
    pcap = round_up(capacity, 16)
    column = width // groups
    here = filtered.shape[1]
    slots = n * pcap
    dma = pltpu.SemaphoreType.DMA
    shape = jax.ShapeDtypeStruct
    gain = expert_gain[None]
    rows, cots, places, stats = call(
        functools.partial(dispatch_kernel, n, groups, pcap),
        0,
        [
            shape((slots, width), BF16),
            shape((slots, width), BF16),
            shape((slots, tokens), BF16),
            shape((groups, 8, tokens), F32),
        ],
        [
            pltpu.VMEM((slots, column), BF16),
            pltpu.VMEM((slots, column), BF16),
            dma((2, n)),
            dma((2, n)),
            dma((2, n, groups)),
            dma((2, n, groups)),
            dma((groups,)),
            dma((groups,)),
        ],
        (
            stream,
            upstream,
            gain,
            expert_ids.T.reshape(1, 2 * tokens),
            group_weight[:, None],
            pair_scores,
            filtered,
        ),
    )
    gate_local, up_local, down_local = gate_weight[0], up_weight[0], down_weight[0]
    pre_gate = jnp.dot(rows, gate_local, preferred_element_type=F32)
    pre_up = jnp.dot(rows, up_local, preferred_element_type=F32)
    sigma = jax.nn.sigmoid(pre_gate)
    silu_gate = pre_gate * sigma
    hidden = (silu_gate * pre_up).astype(BF16)
    grad_hidden = contract_last(cots, down_local)
    grad_pre_gate = (grad_hidden * pre_up * silu_slope(pre_gate, sigma)).astype(BF16)
    grad_pre_up = (grad_hidden * silu_gate).astype(BF16)
    partial = (
        contract_last(grad_pre_gate, gate_local) + contract_last(grad_pre_up, up_local)
    ).astype(BF16)
    gradient_gate = contract_first(rows, grad_pre_gate)[None]
    gradient_up = contract_first(rows, grad_pre_up)[None]
    gradient_down = contract_first(hidden, cots)[None]
    db = width // n
    pdb = round_up(db, 128)
    half = groups // 2
    hpad = round_up(kernel_taps.shape[0] - 1, 16)
    staged = (n, tokens // groups, pdb) if pdb != db else (1, 16, 128)
    gradient_value, gradient_gating, gradient_mixer = call(
        functools.partial(tail_kernel, n, groups, pcap),
        1,
        [
            shape((tokens, here), BF16),
            shape((tokens, here), BF16),
            shape((db, here), F32),
        ],
        [
            pltpu.VMEM((slots, half * column), BF16),
            pltpu.VMEM((slots, half * column), BF16),
            pltpu.VMEM((16, 128), F32),
            pltpu.VMEM((slots, max(1, half - 1) * column), BF16),
            pltpu.VMEM((slots, column), BF16),
            pltpu.VMEM((slots, column), BF16),
            pltpu.VMEM((tokens, width), BF16),
            pltpu.VMEM((tokens, width), BF16),
            pltpu.VMEM(staged, BF16),
            pltpu.VMEM((n * tokens, pdb), BF16),
            pltpu.VMEM((n * tokens, here), BF16),
            pltpu.VMEM((groups, 8, tokens), F32),
            pltpu.VMEM((hpad, here), BF16),
            pltpu.VMEM((hpad, here), BF16),
            pltpu.VMEM((tokens + hpad, here), F32),
            dma((n, half)),
            dma((n, half)),
            dma((n, half)),
            dma((n, half)),
            dma((n,)),
            dma((n,)),
            dma((groups,)),
            dma((groups,)),
            dma((n // 2,)),
            dma((n // 2,)),
            dma((n // 2,)),
            dma((n // 2,)),
            dma((n,)),
            dma((n,)),
            dma((n, groups)),
            dma((n, groups)),
            dma((groups,)),
            dma((groups,)),
            dma(()),
            dma(()),
        ],
        (
            partial,
            places,
            stats,
            stream,
            upstream,
            gain,
            mixer_weight,
            filtered,
            channel_gain[None],
            kernel_taps,
            value_branch,
            gate_branch,
        ),
    )
    return (
        gradient_value,
        gradient_gating,
        gradient_mixer,
        gradient_gate,
        gradient_up,
        gradient_down,
    )


def solution(mesh):
    return jax.shard_map(
        body,
        mesh=mesh,
        in_specs=(
            P("sp", None),
            P("sp", None),
            P(),
            P("sp", None),
            P("sp"),
            P("sp", None),
            P("sp", None, "tp"),
            P("sp", None, "tp"),
            P("sp", "tp", None),
            P("tp", None),
            P("sp", "tp"),
            P("tp"),
            P(None, "tp"),
            P("sp", "tp"),
            P("sp", "tp"),
        ),
        out_specs=(
            P("sp", "tp"),
            P("sp", "tp"),
            P("sp", "tp"),
            P("sp", None, "tp"),
            P("sp", None, "tp"),
            P("sp", "tp", None),
        ),
        check_vma=False,
    )
```

profile of v0, /device:TPU:0, one launch (start us, length us, event | category | flops | bytes accessed | tf_op | source)
XLA Modules:
  0.0 111.9 jit_solution(1085850886223859714)
XLA Ops:
  0.6 0.0 copy-start
  0.6 0.9 copy.22.weight
  1.5 0.8 copy.23.scores
  2.3 0.8 reshape.15.ids
  3.1 0.0 copy-start.1
  3.1 1.1 %copy-done.1 = bf16[192,2048]{1,0:T(8,128)(2,1)S(1)} copy-done((bf16[192,2048]{1,0:T(8,128)(2,1)S(1)}, bf16[192,2048]{1,0:T(8,128)(2,1)}, u32[]{:S(2)}) %copy-start.1) | copy-done | bytes 786456
  4.2 0.0 copy-start.2
  4.2 1.1 %copy-done.2 = bf16[192,2048]{1,0:T(8,128)(2,1)S(1)} copy-done((bf16[192,2048]{1,0:T(8,128)(2,1)S(1)}, bf16[192,2048]{1,0:T(8,128)(2,1)}, u32[]{:S(2)}) %copy-start.2) | copy-done | bytes 786456
  5.4 0.0 copy-start.4
  5.4 0.9 copy-done.4
  6.3 0.0 copy-start.9
  6.3 0.7 copy-done.9
  7.0 40.1 %shard_map.190 = (bf16[512,2048]{1,0:T(8,128)(2,1)S(1)}, bf16[512,2048]{1,0:T(8,128)(2,1)S(1)}, bf16[512,192]{1,0:T(8,128)(2,1)S(1)}, f32[4,8,192]{2,1,0:T(8,128)S(1)}) custom-call(bf16[192,2048]{1,0:T(8,128)(2,1)S(1)} %copy-done.1, bf16[192,2048]{1,0:T(8,128)(2,1)S(1)} %copy-done.2, f32[1,2048]{1,0:T(1,128)S(1)} %bitcast.35, s32[1,384]{1,0:T(1,128)S(1)} %reshape.15.ids, ...), custom_call_target="tpu_custom_call" | custom-call | tf_op jit(solution)/shard_map/pallas_call | solution.py:609
  47.1 0.0 copy-start.11
  47.1 0.0 copy-done
  47.1 0.7 fusion.2
  47.8 0.5 copy-done.11
  48.3 0.0 copy-start.12
  48.3 0.7 fusion.5
  49.0 0.5 copy-done.12
  49.5 0.9 multiply_convert_fusion.1
  50.4 0.7 fusion
  51.2 0.0 copy-start.3
  51.2 0.0 copy-start.5
  51.2 0.0 copy-start.6
  51.2 0.0 copy-start.7
  51.2 0.0 copy-start.8
  51.2 0.0 copy-start.10
  51.2 0.7 add_convert_fusion.partial
  52.0 0.4 copy-done.3
  52.4 0.0 copy-done.5
  52.4 0.0 copy-done.6
  52.4 0.0 copy-done.7
  52.4 0.0 copy-done.8
  52.4 0.0 copy-done.10
  52.4 51.3 %shard_map.191 = (bf16[192,256]{1,0:T(8,128)(2,1)S(1)}, bf16[192,256]{1,0:T(8,128)(2,1)S(1)}, f32[256,256]{1,0:T(8,128)S(1)}) custom-call(bf16[512,2048]{1,0:T(8,128)(2,1)S(1)} %add_convert_fusion.partial, bf16[512,192]{1,0:T(8,128)(2,1)S(1)} %get-tuple-element.15.places, f32[4,8,192]{2,1,0:T(8,128)S(1)} %get-tuple-element.16.stats, ...), custom_call_target="tpu_custom_call" | custom-call | tf_op jit(solution)/shard_map/pallas_call | solution.py:609
  103.7 2.1 %convolution_bitcast_fusion.1 = f32[1,2048,256]{2,1,0:T(8,128)} fusion(bf16[512,2048]{1,0:T(8,128)(2,1)S(1)} %get-tuple-element.14, bf16[512,256]{1,0:T(8,128)(2,1)S(1)} %get-tuple-element.20), kind=kOutput, calls=%fused_computation.2 | convolution fusion | flops 536870912 | bytes 4456448 | tf_op jit(solution)/shard_map/dot_general | solution.py:28
  105.8 2.1 %convolution_bitcast_fusion.2 = f32[1,2048,256]{2,1,0:T(8,128)} fusion(bf16[512,2048]{1,0:T(8,128)(2,1)S(1)} %get-tuple-element.14, bf16[512,256]{1,0:T(8,128)(2,1)S(1)} %get-tuple-element.21), kind=kOutput, calls=%fused_computation.3 | convolution fusion | flops 536870912 | bytes 4456448 | tf_op jit(solution)/shard_map/dot_general | solution.py:28
  107.8 2.1 %convolution_bitcast_fusion = f32[1,256,2048]{2,1,0:T(8,128)} fusion(bf16[512,2048]{1,0:T(8,128)(2,1)S(1)} %get-tuple-element.13, f32[512,256]{1,0:T(8,128)S(1)} %fusion.5, f32[512,256]{1,0:T(8,128)S(1)} %fusion.2), kind=kOutput, calls=%fused_computation.1 | convolution fusion | flops 537657344 | bytes 5242880 | tf_op jit(solution)/shard_map/dot_general | solution.py:28
  109.9 0.6 copy.27
  110.6 0.6 copy.28
  111.2 0.7 copy.29
Async XLA Ops:
  0.6 46.5 %copy-start = (bf16[1,2048,256]{2,1,0:T(8,128)(2,1)S(1)}, bf16[1,2048,256]{2,1,0:T(8,128)(2,1)}, u32[]{:S(2)}) copy-start(bf16[1,2048,256]{2,1,0:T(8,128)(2,1)} %param.21) | copy-start | bytes 3145732
  3.1 1.1 %copy-start.1 = (bf16[192,2048]{1,0:T(8,128)(2,1)S(1)}, bf16[192,2048]{1,0:T(8,128)(2,1)}, u32[]{:S(2)}) copy-start(bf16[192,2048]{1,0:T(8,128)(2,1)} %stream.3) | copy-start | bytes 2359300
  4.2 1.1 %copy-start.2 = (bf16[192,2048]{1,0:T(8,128)(2,1)S(1)}, bf16[192,2048]{1,0:T(8,128)(2,1)}, u32[]{:S(2)}) copy-start(bf16[192,2048]{1,0:T(8,128)(2,1)} %upstream.3) | copy-start | bytes 2359300
  5.4 0.9 copy-start.4
  6.3 0.7 copy-start.9
  47.1 1.2 %copy-start.11 = (bf16[1,2048,256]{2,1,0:T(8,128)(2,1)S(1)}, bf16[1,2048,256]{2,1,0:T(8,128)(2,1)}, u32[]{:S(2)}) copy-start(bf16[1,2048,256]{2,1,0:T(8,128)(2,1)} %param.22) | copy-start | bytes 3145732
  48.3 1.2 %copy-start.12 = (bf16[1,256,2048]{2,1,0:T(8,128)(2,1)S(1)}, bf16[1,256,2048]{2,1,0:T(8,128)(2,1)}, u32[]{:S(2)}) copy-start(bf16[1,256,2048]{2,1,0:T(8,128)(2,1)} %param.23) | copy-start | bytes 3145732
  51.2 1.2 %copy-start.3 = (bf16[256,2048]{1,0:T(8,128)(2,1)S(1)}, bf16[256,2048]{1,0:T(8,128)(2,1)}, u32[]{:S(2)}) copy-start(bf16[256,2048]{1,0:T(8,128)(2,1)} %mixer.1) | copy-start | bytes 3145732
  51.2 1.2 %copy-start.5 = (bf16[192,256]{1,0:T(8,128)(2,1)S(1)}, bf16[192,256]{1,0:T(8,128)(2,1)}, u32[]{:S(2)}) copy-start(bf16[192,256]{1,0:T(8,128)(2,1)} %filtered.3) | copy-start | bytes 294916
  51.2 1.2 %copy-start.6 = (bf16[192,256]{1,0:T(8,128)(2,1)S(1)}, bf16[192,256]{1,0:T(8,128)(2,1)}, u32[]{:S(2)}) copy-start(bf16[192,256]{1,0:T(8,128)(2,1)} %value.1) | copy-start | bytes 294916
  51.2 1.2 %copy-start.7 = (bf16[192,256]{1,0:T(8,128)(2,1)S(1)}, bf16[192,256]{1,0:T(8,128)(2,1)}, u32[]{:S(2)}) copy-start(bf16[192,256]{1,0:T(8,128)(2,1)} %gate.1) | copy-start | bytes 294916
  51.2 1.2 %copy-start.8 = (f32[31,256]{1,0:T(8,128)S(1)}, f32[31,256]{1,0:T(8,128)}, u32[]{:S(2)}) copy-start(f32[31,256]{1,0:T(8,128)} %taps.1) | copy-start | bytes 95236
  51.2 1.2 %copy-start.10 = (f32[256]{0:T(256)S(1)}, f32[256]{0:T(256)}, u32[]{:S(2)}) copy-start(f32[256]{0:T(256)} %param.26) | copy-start | bytes 3076
where the time goes:
time: 112 us
  Pallas kernels  91.4 us (82%)
  matrix products  10 us (9%)
  local copies, waits for them, and re-layouts  9.75 us (9%)
    pallas_call x2, Pallas kernels, call(): pl.pallas_call(kernel, out_shape=outs, in_specs=[pl.BlockSpec(memory_spac...  91.4 us
    unnamed x30, local copies, waits for them, and re-layouts  8.1 us
    dot_general x3, matrix products, contract_first(): lax.dot_general(left, right, (((0,), (0,)), ((), ())), preferred_element_...  6.22 us
    dot_general x3, matrix products, contract_last(): lax.dot_general(left, right, (((1,), (1,)), ((), ())), preferred_element_...  2.37 us

commit v1 on v0

v1 whole, which is shorter than its diff:
```python
import functools

import jax
import jax.numpy as jnp
from jax import lax
from jax.experimental import pallas as pl
from jax.experimental.pallas import tpu as pltpu
from jax.sharding import PartitionSpec as P

EPS = 1e-06
MESH = pl.DeviceIdType.MESH
F32 = jnp.float32
BF16 = jnp.bfloat16
HIGHEST = lax.Precision.HIGHEST
UNROLL = 8
DIRECT = 2


def silu_slope(value, sigma):
    return sigma * (1.0 + value * (1.0 - sigma))


def contract_last(left, right, precision=None):
    return lax.dot_general(
        left, right, (((1,), (1,)), ((), ())), preferred_element_type=F32, precision=precision
    )


def contract_first(left, right):
    return lax.dot_general(left, right, (((0,), (0,)), ((), ())), preferred_element_type=F32)


def dot(left, right):
    return jnp.dot(left, right, preferred_element_type=F32)


def round_up(value, unit):
    return -(-value // unit) * unit


def flip(index, mask):
    bit = 1
    while bit <= mask:
        if mask & bit:
            index = index + bit - 2 * bit * ((index // bit) % 2)
        bit *= 2
    return index


def either(index, mask, limit):
    if isinstance(mask, int):
        return flip(index, mask)
    bit, total = 1, 0
    while bit < limit:
        total = total + bit * (((index // bit) % 2 + (mask // bit) % 2) % 2)
        bit *= 2
    return total


def low_bit(mask):
    return mask & -mask


def bits_below(limit):
    found, bit = [], 1
    while bit < limit:
        found.append(bit)
        bit *= 2
    return found[::-1]


def remote(src, dst, send, recv, where):
    return pltpu.make_async_remote_copy(
        src_ref=src, dst_ref=dst, send_sem=send, recv_sem=recv, device_id=where, device_id_type=MESH
    )


def start_of(i, unit):
    return i * unit if isinstance(i, int) else pl.multiple_of(i * unit, unit)


class Spread:
    def __init__(self, axis, place, index, count, send, recv):
        self.axis, self.place, self.index, self.count = axis, place, index, count
        self.send_sem, self.recv_sem = send, recv

    def copy(self, mask, bit):
        ref = self.place(flip(self.index, mask))
        return remote(
            ref,
            ref,
            self.send_sem(mask | bit),
            self.recv_sem(mask | bit),
            {self.axis: flip(self.index, bit)},
        )

    def wait(self, mask):
        ref = self.place(flip(self.index, mask))
        where = {self.axis: flip(self.index, low_bit(mask))}
        remote(ref, ref, self.send_sem(mask), self.recv_sem(mask), where).wait_recv()

    def begin(self):
        for bit in bits_below(self.count):
            self.copy(0, bit).start()

    def masks(self):
        return sorted(range(1, self.count), key=lambda m: (bin(m).count("1"), -low_bit(m)))

    def relay(self):
        for mask in self.masks():
            onward = bits_below(low_bit(mask))
            if onward:
                self.wait(mask)
                for bit in onward:
                    self.copy(mask, bit).start()

    def arrived(self):
        for mask in self.masks():
            if not bits_below(low_bit(mask)):
                self.wait(mask)

    def sent(self):
        for mask in range(1, self.count):
            self.copy(mask - low_bit(mask), low_bit(mask)).wait_send()


class Direct:
    def __init__(self, place, index, count, send, recv):
        self.place, self.index, self.count = place, index, count
        self.send_sem, self.recv_sem = send, recv

    def copy(self, mask, origin):
        ref = self.place(origin)
        return remote(
            ref, ref, self.send_sem.at[mask], self.recv_sem.at[mask], {"tp": flip(self.index, mask)}
        )

    def begin(self):
        for mask in range(1, self.count):
            self.copy(mask, self.index).start()

    def arrived(self):
        for mask in range(1, self.count):
            self.copy(mask, flip(self.index, mask)).wait_recv()

    def sent(self):
        for mask in range(1, self.count):
            self.copy(mask, self.index).wait_send()


def bands_of(n):
    sizes = (n // 4, n // 4, n // 4, n // 8, n // 8)
    found, first = [], 0
    for size in sizes:
        found.append((first, first + size))
        first += size
    return found


def direct_of(n):
    return n // DIRECT


def each(first, last, step):
    if last - first <= UNROLL:
        for i in range(first, last):
            step(i)
        return

    def run(i, carry):
        step(i)
        return carry

    lax.fori_loop(first, last, run, 0)


INPUTS = (
    "ids",
    "weight",
    "scores",
    "gain",
    "stream",
    "upstream",
    "filtered",
    "gate_w",
    "up_w",
    "down_w",
    "channel_gain",
    "mixer",
    "taps",
    "value",
    "gate",
)
OUTPUTS = ("out_value", "out_gating", "out_mixer", "out_gate", "out_up", "out_down")


def layer_kernel(n, groups, pcap, names, *refs):
    r = dict(zip(names, refs))
    v = {name: r["v_" + name] for name in INPUTS}
    me, tp = lax.axis_index("sp"), lax.axis_index("tp")
    tokens, width = v["stream"].shape
    column = width // groups
    here = v["filtered"].shape[1]
    channels = here * groups
    slots = n * pcap
    portion = tokens // groups
    db = width // n
    pdb = r["grad_all"].shape[1]
    reach = v["taps"].shape[0] - 1
    hpad = r["halo_in"].shape[0]
    bands = bands_of(n)
    near = direct_of(n)
    top = n // 2
    half = groups // 2
    scope = jax.named_scope

    def peer(m):
        return either(me, m, n)

    barrier = pltpu.get_barrier_semaphore()
    each(
        1,
        n,
        lambda m: pl.semaphore_signal(
            barrier, inc=1, device_id={"sp": peer(m)}, device_id_type=MESH
        ),
    )
    for k in range(1, groups):
        pl.semaphore_signal(barrier, inc=1, device_id={"tp": flip(tp, k)}, device_id_type=MESH)
    before = lax.rem(me + n - 1, n)

    def load(name):
        return pltpu.make_async_copy(r[name], v[name], r["load"].at[INPUTS.index(name)])

    for name in INPUTS:
        load(name).start()

    with scope("slots"):
        earlier = (
            (
                lax.broadcasted_iota(jnp.int32, (tokens, tokens), 0)
                < lax.broadcasted_iota(jnp.int32, (tokens, tokens), 1)
            )
            .astype(F32)
            .astype(BF16)
        )
        eye = (
            lax.broadcasted_iota(jnp.int32, (tokens, tokens), 0)
            == lax.broadcasted_iota(jnp.int32, (tokens, tokens), 1)
        ).astype(F32)
        block_id = lax.broadcasted_iota(jnp.int32, (n, tokens), 0)
        expert = jnp.bitwise_xor(block_id, me)
        slot_at = lax.broadcasted_iota(jnp.int32, (slots, tokens), 0)
        load("ids").wait()
        hit_a = (expert == v["ids"][0:1]).astype(F32)
        hit_b = (expert == v["ids"][1:2]).astype(F32)
        ahead_a = dot(hit_a.astype(BF16), earlier)
        ahead_b = dot(hit_b.astype(BF16), earlier) + jnp.sum(hit_a, axis=1, keepdims=True)
        base = (block_id * pcap).astype(F32)
        slot_a = jnp.sum(hit_a * (ahead_a + base), axis=0, keepdims=True)
        slot_b = jnp.sum(hit_b * (ahead_b + base), axis=0, keepdims=True)
        first = (slot_at == slot_a.astype(jnp.int32)).astype(F32).astype(BF16)
        second = (slot_at == slot_b.astype(jnp.int32)).astype(F32).astype(BF16)
        both = first + second
        r["first"][...] = first
        r["second"][...] = second
        for name in ("weight", "scores", "gain"):
            load(name).wait()
        spread = v["scores"][0:1] - v["scores"][1:2]
        weight_a = v["weight"][...] * jax.nn.sigmoid(spread)
        weight_b = v["weight"][...] * jax.nn.sigmoid(-spread)
        line = lax.broadcasted_iota(jnp.int32, (8, tokens), 0)
        small = jnp.where(
            line == 0,
            weight_a,
            jnp.where(line == 1, weight_b, jnp.where(line == 2, slot_a, slot_b)),
        )
        small = contract_last(eye, small, HIGHEST)
        weight_a, weight_b = small[:, 0:1], small[:, 1:2]
        slot_col_a = small[:, 2:3].astype(jnp.int32)
        slot_col_b = small[:, 3:4].astype(jnp.int32)

    with scope("rows"):
        load("stream").wait()
        load("upstream").wait()
        inv_rms = jnp.zeros((tokens, 1), F32)
        for q in range(groups):
            piece = v["stream"][:, q * column : (q + 1) * column].astype(F32)
            inv_rms = inv_rms + jnp.sum(piece * piece, axis=1, keepdims=True)
        inv_rms = lax.rsqrt(inv_rms / width + EPS)

        def quarter(q):
            return pl.ds(start_of(q, column), column)

        def routed(cols, rows):
            normed = (v["stream"][:, cols].astype(F32) * inv_rms * v["gain"][:, cols]).astype(BF16)
            up = v["upstream"][:, cols].astype(F32)
            scaled_a = (weight_a * up).astype(BF16)
            scaled_b = (weight_b * up).astype(BF16)
            one, two = r["first"][rows], r["second"][rows]
            return (
                dot(one + two, normed).astype(BF16),
                (dot(one, scaled_a) + dot(two, scaled_b)).astype(BF16),
            )

        mine_q = quarter(tp)
        side = lax.rem(tp, 2)

        def lane_q(h):
            return quarter(side + 2 * h)

        def stage(cols, lo, hi, at, rows_to, cots_to):
            out_rows, out_cots = routed(cols, slice(lo * pcap, hi * pcap))
            rows_to[at] = out_rows
            cots_to[at] = out_cots

        for h in range(half):
            at = (slice(0, (near - 1) * pcap), slice(h * column, (h + 1) * column))
            stage(lane_q(h), 1, near, at, r["near_rows"], r["near_cots"])

    pairs = ((r["send_rows"], r["rows"]), (r["send_cots"], r["cots"]))
    close = (r["near_rows"], r["near_cots"])

    def block(m):
        return pl.ds(start_of(m, pcap), pcap)

    def near_copy(a, m, h):
        return remote(
            close[a].at[block(m - 1), pl.ds(h * column, column)],
            pairs[a][1].at[block(m), lane_q(h)],
            r["near_send"].at[a, m, h],
            r["near_recv"].at[a, m, h],
            {"sp": peer(m)},
        )

    def core_share(a, m, h):
        ref = pairs[a][1].at[block(m), lane_q(h)]
        return remote(
            ref, ref, r["share_send"].at[a, m, h], r["share_recv"].at[a, m, h], {"tp": flip(tp, 1)}
        )

    def sp_copy(a, m):
        src, full = pairs[a]
        return remote(
            src.at[block(m - near)],
            full.at[block(m), mine_q],
            r["sp_send"].at[a, m],
            r["sp_recv"].at[a, m],
            {"sp": peer(m)},
        )

    with scope("barrier"):
        pl.semaphore_wait(barrier, n - 1 + groups - 1)

    def send_near(m):
        for a in range(2):
            for h in range(half):
                near_copy(a, m, h).start()

    def send(m):
        for a in range(2):
            sp_copy(a, m).start()

    def send_any(lo, hi):
        each(lo, min(hi, near), send_near)
        each(max(lo, near), hi, send)

    parts = ((1, n // 4), (n // 2, 3 * n // 4), (n // 4, n // 2), (3 * n // 4, n))
    send_any(*parts[0])
    with scope("rows2"):
        stage(mine_q, near, n, slice(0, (n - near) * pcap), r["send_rows"], r["send_cots"])
    for lo, hi in parts[1:]:
        send_any(lo, hi)

    with scope("stats"):
        load("filtered").wait()
        filt = v["filtered"][...]
        square = filt.astype(F32) * filt.astype(F32)
        high = square.astype(BF16)
        low = (square - high.astype(F32)).astype(BF16)
        ones = jnp.ones((8, here), BF16)
        total = contract_last(ones, filt)
        total_square = contract_last(ones, high) + contract_last(ones, low)
        r["stats"][tp] = jnp.where(line == 0, total, total_square)
        sums = Direct(lambda o: r["stats"].at[o], tp, groups, r["st_send"], r["st_recv"])
        sums.begin()

    with scope("own"):
        for q in range(groups):
            cols = slice(q * column, (q + 1) * column)
            own_rows, own_cots = routed(cols, slice(0, pcap))
            r["rows"][0:pcap, cols] = own_rows
            r["cots"][0:pcap, cols] = own_cots
        lane = lax.broadcasted_iota(jnp.int32, (tokens, slots), 1)
        r["places"][...] = (
            ((lane == slot_col_a) | (lane == slot_col_b)).astype(F32).astype(BF16)
        )

    def gather(a, m):
        return Spread(
            "tp",
            lambda o: pairs[a][1].at[block(m), quarter(o)],
            tp,
            groups,
            lambda k: r["tp_send"].at[a, m, k],
            lambda k: r["tp_recv"].at[a, m, k],
        )

    def arrive_near(m):
        for a in range(2):
            for h in range(half):
                near_copy(a, m, h).wait_recv()
                core_share(a, m, h).start()

    def arrived_near(m):
        for a in range(2):
            for h in range(half):
                core_share(a, m, h).wait_recv()

    def arrive(m):
        for a in range(2):
            sp_copy(a, m).wait_recv()
            gather(a, m).begin()

    def relay(m):
        for a in range(2):
            gather(a, m).relay()

    def arrived(m):
        for a in range(2):
            gather(a, m).arrived()

    def band(c):
        return pl.ds(bands[c][0] * pcap, (bands[c][1] - bands[c][0]) * pcap)

    wide = 2 * v["gate_w"].shape[1]
    turned = wide // 2

    def turn():
        tile = min(256, width)
        for t in range(0, width, tile):
            at = slice(t, t + tile)
            for k, name in enumerate(("gate_w", "up_w")):
                r["back_w"][k * turned : (k + 1) * turned, at] = v[name][at].T
            r["down_t"][at] = v["down_w"][:, at].T

    def compute(c):
        at = band(c)
        rows, cots = r["rows"][at], r["cots"][at]
        pre_gate = dot(rows, v["gate_w"][...])
        pre_up = dot(rows, v["up_w"][...])
        grad_hidden = dot(cots, r["down_t"][...])
        sigma = jax.nn.sigmoid(pre_gate)
        silu_gate = pre_gate * sigma
        grad_pre_gate = (grad_hidden * pre_up * silu_slope(pre_gate, sigma)).astype(BF16)
        grad_pre_up = (grad_hidden * silu_gate).astype(BF16)
        r["hidden"][at] = (silu_gate * pre_up).astype(BF16)
        r["gpg"][at] = grad_pre_gate
        r["gpu"][at] = grad_pre_up
        slopes_in = jnp.concatenate([grad_pre_gate, grad_pre_up], axis=1)
        for q in range(groups):
            cols = slice(q * column, (q + 1) * column)
            r["partial"][at, cols] = dot(slopes_in, r["back_w"][:, cols]).astype(BF16)

    mate = flip(tp, 1)
    mine = tp // 2

    def core_copy(c, h):
        return remote(
            r["partial"].at[band(c), quarter(lax.rem(mate, 2) + 2 * h)],
            r["halves"].at[band(c), pl.ds(h * column, column)],
            r["core_send"].at[c, h],
            r["core_recv"].at[c, h],
            {"tp": mate},
        )

    def cross(c, k):
        return remote(
            r["passing"].at[band(c), quarter(flip(mine, k))],
            r["crossed"].at[band(c), pl.ds((k - 1) * column, column)],
            r["x_send"].at[c, k],
            r["x_recv"].at[c, k],
            {"tp": flip(tp, 2 * k)},
        )

    def start_core(c):
        for h in range(half):
            core_copy(c, h).start()

    def add_core(c):
        for h in range(half):
            core_copy(c, h).wait_recv()
        for h in range(half):
            cols = pl.ds(h * column, column)
            own = r["partial"][band(c), quarter(lax.rem(tp, 2) + 2 * h)].astype(F32)
            r["passing"][band(c), cols] = (
                own + r["halves"][band(c), cols].astype(F32)
            ).astype(BF16)
        for k in range(1, half):
            cross(c, k).start()

    def home_copy(m):
        return remote(
            r["outgoing"].at[block(m)],
            r["back"].at[block(m)],
            r["home_send"].at[m],
            r["home_recv"].at[m],
            {"sp": peer(m)},
        )

    def add_cross(c):
        for k in range(1, half):
            cross(c, k).wait_recv()
        total = r["passing"][band(c), quarter(mine)].astype(F32)
        for k in range(1, half):
            total = total + r["crossed"][band(c), pl.ds((k - 1) * column, column)].astype(F32)
        r["outgoing"][band(c)] = total.astype(BF16)
        each(max(1, bands[c][0]), bands[c][1], lambda m: home_copy(m).start())

    def act_rows(s):
        return pl.ds(start_of(s, tokens), tokens)

    acts = Spread(
        "sp",
        lambda o: r["act_all"].at[act_rows(o)],
        me,
        n,
        lambda m: r["act_send"].at[m],
        lambda m: r["act_recv"].at[m],
    )

    def early(bit):
        acts.copy(0, bit).start()

    def arrivals(lo, hi):
        with scope("arrive#m=%d" % lo):
            each(lo, min(hi, near), arrive_near)

            def step(m):
                arrive(m)
                if isinstance(m, int):
                    if m > max(lo, near):
                        relay(m - 1)
                else:
                    pl.when(m > max(lo, near))(lambda: relay(m - 1))

            each(max(lo, near), hi, step)

    def lastrelay(hi):
        if hi > near:
            with scope("relay#m=%d" % (hi - 1)):
                relay(hi - 1)

    def whole(c):
        lo, hi = bands[c]
        with scope("finish#c=%d" % c):
            each(max(1, lo), min(hi, near), arrived_near)
            each(max(1, lo, near), hi, arrived)
        with scope("compute#c=%d" % c):
            compute(c)
            start_core(c)

    with scope("turn"):
        for name in ("gate_w", "up_w", "down_w"):
            load(name).wait()
        turn()
    with scope("normact"):
        sums.arrived()
        moments = r["stats"][0]
        for o in range(1, groups):
            moments = moments + r["stats"][o]
        moments = contract_last(eye, moments, HIGHEST)
        mean_c = moments[:, 0:1] / channels
        variance = moments[:, 1:2] / channels - mean_c * mean_c
        inv_std = lax.rsqrt(variance + EPS)
        load("channel_gain").wait()

        def norms():
            centred = (v["filtered"][...].astype(F32) - mean_c) * inv_std
            normal_out = centred * v["channel_gain"][...]
            return centred, normal_out, jax.nn.sigmoid(normal_out)

        _, normal_out, sig_norm = norms()
        r["act_all"][act_rows(me)] = (normal_out * sig_norm).astype(BF16)

    def addcore(c):
        with scope("addcore#c=%d" % c):
            add_core(c)

    def addcross(c):
        with scope("addcross#c=%d" % c):
            add_cross(c)

    def act_relay(masks):
        for mask in masks:
            onward = bits_below(low_bit(mask))
            if onward:
                acts.wait(mask)
                for bit in onward:
                    acts.copy(mask, bit).start()

    act_masks = acts.masks()
    quarter_n, last = n // 4, len(bands) - 1
    one, two, three = bands[1][0], bands[2][0], bands[3][0]
    final = bands[4][0]
    arrivals(1, one)
    lastrelay(one)
    whole(0)
    arrivals(two, three)
    addcore(0)
    lastrelay(three)
    whole(2)
    addcross(0)
    arrivals(one, two)
    addcore(2)
    lastrelay(two)
    whole(1)
    arrivals(three, final)
    addcore(1)
    addcross(2)
    arrivals(final, n)
    lastrelay(final)
    whole(3)
    for bit in bits_below(n):
        early(bit)
    lastrelay(n)
    addcross(1)
    addcore(3)
    whole(4)
    addcross(3)
    addcore(4)

    tile = min(256, width)

    def wgrad(left, pick):
        def step(t):
            cols = pl.ds(start_of(t, tile), tile)
            r[pick][cols] = contract_first(r["rows"][:, cols], r[left][...])

        lax.fori_loop(0, width // tile, lambda t, c: (step(t), c)[1], 0)

    def wgrad_down():
        def step(t):
            cols = pl.ds(start_of(t, tile), tile)
            r["out_down"][:, cols] = contract_first(r["hidden"][...], r["cots"][:, cols])

        lax.fori_loop(0, width // tile, lambda t, c: (step(t), c)[1], 0)

    with scope("wgrad_gate"):
        wgrad("gpg", "out_gate")
    with scope("addcross#c=%d" % last):
        add_cross(last)
        r["back"][0:pcap] = r["outgoing"][0:pcap]
    with scope("wgrad_up"):
        wgrad("gpu", "out_up")
    with scope("home"):
        each(1, n, lambda m: home_copy(m).wait_recv())
    with scope("combine"):
        r["grad_normed"][:, mine_q] = dot(r["places"][...], r["back"][...]).astype(BF16)
        normal = Spread(
            "tp",
            lambda o: r["grad_normed"].at[:, quarter(o)],
            tp,
            groups,
            lambda m: r["gn_send"].at[m],
            lambda m: r["gn_recv"].at[m],
        )
        normal.begin()
    with scope("actrelay2"):
        act_relay([m for m in act_masks if m <= top])
    with scope("wgrad_down"):
        wgrad_down()
    with scope("actrelay3"):
        act_relay([m for m in act_masks if m > top])
    with scope("gather"):
        normal.relay()
        normal.arrived()

    with scope("gradstream"):
        inner = jnp.zeros((tokens, 1), F32)
        for q in range(groups):
            at = slice(q * column, (q + 1) * column)
            weighted = r["grad_normed"][:, at].astype(F32) * v["gain"][:, at]
            inner = inner + jnp.sum(
                weighted * v["stream"][:, at].astype(F32), axis=1, keepdims=True
            )
        inner = inv_rms * inv_rms * inv_rms * (inner / width)
        for q in range(groups):
            at = slice(q * column, (q + 1) * column)
            weighted = r["grad_normed"][:, at].astype(F32) * v["gain"][:, at]
            r["grad_stream"][:, at] = (
                v["upstream"][:, at].astype(F32)
                + inv_rms * weighted
                - v["stream"][:, at].astype(F32) * inner
            ).astype(BF16)

    def part(s, o):
        start = pl.multiple_of(s * tokens + o * portion, portion)
        return r["grad_all"].at[pl.ds(start, portion)]

    my_rows = pl.ds(pl.multiple_of(tp * portion, portion), portion)
    if db == pdb:

        def cut(j):
            return r["grad_stream"].at[my_rows, pl.ds(pl.multiple_of(j * db, db), db)]

        r["grad_all"][act_rows(me)] = r["grad_stream"][
            :, pl.ds(pl.multiple_of(me * db, db), db)
        ]
    else:

        def pick(j):
            where = lax.broadcasted_iota(jnp.int32, (width, pdb), 0)
            lane = lax.broadcasted_iota(jnp.int32, (width, pdb), 1)
            return ((where == lane + j * db) & (lane < db)).astype(F32).astype(BF16)

        def stage(j):
            r["staged"][j] = dot(r["grad_stream"][my_rows], pick(j)).astype(BF16)

        each(0, n, stage)

        def cut(j):
            return r["staged"].at[j]

        r["grad_all"][act_rows(me)] = dot(r["grad_stream"][...], pick(me)).astype(BF16)

    def cut_copy(m, j, s):
        return remote(cut(j), part(s, tp), r["gs_send"].at[m], r["gs_recv"].at[m], {"sp": j})

    def spread_cut(m):
        s = peer(m)
        return Spread(
            "tp",
            lambda o: part(s, o),
            tp,
            groups,
            lambda k: r["ga_send"].at[m, k],
            lambda k: r["ga_recv"].at[m, k],
        )

    def cut_arrives(m):
        cut_copy(m, peer(m), peer(m)).wait_recv()
        spread_cut(m).begin()

    with scope("cutstart"):
        each(1, n, lambda m: cut_copy(m, peer(m), me).start())

    with scope("slopes"):
        load("mixer").wait()
        grad_act = contract_last(r["grad_stream"][...], v["mixer"][...])
        centred, normal_out, sig_norm = norms()
        grad_centred = grad_act * silu_slope(normal_out, sig_norm) * v["channel_gain"][...]
        ones = jnp.ones((8, here), F32)
        slope_sum = contract_last(ones, grad_centred, HIGHEST)
        slope_cross = contract_last(ones, grad_centred * centred, HIGHEST)
        r["slopes"][tp] = jnp.where(line == 0, slope_sum, slope_cross)
        meet = Direct(lambda o: r["slopes"].at[o], tp, groups, r["sl_send"], r["sl_recv"])
        meet.begin()
    with scope("cutarrive1"):
        each(1, top, cut_arrives)
    with scope("meet"):
        meet.arrived()
    with scope("gradfiltered"):
        sums_b = r["slopes"][0]
        for o in range(1, groups):
            sums_b = sums_b + r["slopes"][o]
        sums_b = contract_last(eye, sums_b, HIGHEST)
        grad_filtered = (
            inv_std
            * (grad_centred - sums_b[:, 0:1] / channels - centred * (sums_b[:, 1:2] / channels))
        ).astype(BF16)
        r["halo_out"][...] = grad_filtered[:hpad]
        r["ext"][:tokens] = grad_filtered.astype(F32)

        def halo_copy():
            return remote(
                r["halo_out"], r["halo_in"], r["halo_send"], r["halo_recv"], {"sp": before}
            )

        halo_copy().start()

    def conv(lo, hi):
        mixed = jnp.zeros((hi - lo, here), F32)
        for k in range(reach + 1):
            mixed = mixed + v["taps"][k : k + 1] * r["ext"][lo + reach - k : hi + reach - k]
        sig_gate = jax.nn.sigmoid(v["gate"][lo:hi].astype(F32))
        r["out_value"][lo:hi] = (mixed * sig_gate).astype(BF16)
        r["out_gating"][lo:hi] = (
            mixed * v["value"][lo:hi].astype(F32) * sig_gate * (1.0 - sig_gate)
        ).astype(BF16)

    with scope("cutarrive2"):
        each(top, n - n // 4, cut_arrives)
    with scope("conv1"):
        for name in ("taps", "value", "gate"):
            load(name).wait()
        conv(0, tokens - hpad)
    with scope("cutarrive3"):
        each(n - n // 4, n, cut_arrives)
    with scope("halo"):
        halo_copy().wait_recv()
        inside = jnp.where(me < n - 1, 1.0, 0.0)
        r["ext"][tokens:] = r["halo_in"][...].astype(F32) * inside
    with scope("conv2"):
        conv(tokens - hpad, tokens)
    with scope("cutrelay"):
        each(1, n, lambda m: spread_cut(m).relay())
    with scope("cutwait"):
        each(1, n, lambda m: spread_cut(m).arrived())
    with scope("actwait"):
        acts.arrived()
    with scope("mixer"):
        r["out_mixer"][...] = contract_first(r["grad_all"][...], r["act_all"][...])[:db]

    with scope("drain"):

        def sent(m):
            home_copy(m).wait_send()
            cut_copy(m, peer(m), me).wait_send()
            spread_cut(m).sent()

        def sent_near(m):
            for a in range(2):
                for h in range(half):
                    near_copy(a, m, h).wait_send()
                    core_share(a, m, h).wait_send()

        def sent_far(m):
            for a in range(2):
                sp_copy(a, m).wait_send()
                gather(a, m).sent()

        each(1, near, sent_near)
        each(near, n, sent_far)
        each(1, n, sent)
        sums.sent()
        normal.sent()
        meet.sent()
        acts.sent()
        halo_copy().wait_send()
        for c in range(len(bands)):
            for h in range(half):
                core_copy(c, h).wait_send()
            for k in range(1, half):
                cross(c, k).wait_send()


def flush_kernel(*refs):
    count = len(refs) // 2
    sems = refs[-1]
    copies = [
        pltpu.make_async_copy(refs[i], refs[count + i], sems.at[i]) for i in range(count)
    ]
    for copy in copies:
        copy.start()
    for copy in copies:
        copy.wait()


def body(
    stream,
    upstream,
    expert_gain,
    expert_ids,
    group_weight,
    pair_scores,
    gate_weight,
    up_weight,
    down_weight,
    mixer_weight,
    filtered,
    channel_gain,
    kernel_taps,
    value_branch,
    gate_branch,
):
    n, groups = lax.axis_size("sp"), lax.axis_size("tp")
    tokens, width = stream.shape
    capacity = max(2, 5 * tokens // (2 * n))
    pcap = round_up(capacity, 16)
    column = width // groups
    here = filtered.shape[1]
    hidden = gate_weight.shape[2]
    slots = n * pcap
    half = groups // 2
    db = width // n
    pdb = round_up(db, 128)
    hpad = round_up(kernel_taps.shape[0] - 1, 16)
    staged = (n, tokens // groups, pdb) if pdb != db else (1, 16, 128)
    chunks = len(bands_of(n))
    near = direct_of(n)
    dma = pltpu.SemaphoreType.DMA
    shape = jax.ShapeDtypeStruct
    inputs = dict(
        ids=expert_ids.T,
        weight=group_weight[None],
        scores=pair_scores.T,
        gain=expert_gain[None],
        stream=stream,
        upstream=upstream,
        filtered=filtered,
        gate_w=gate_weight[0],
        up_w=up_weight[0],
        down_w=down_weight[0],
        channel_gain=channel_gain[None],
        mixer=mixer_weight,
        taps=kernel_taps,
        value=value_branch,
        gate=gate_branch,
    )
    outs = dict(
        out_value=shape((tokens, here), BF16),
        out_gating=shape((tokens, here), BF16),
        out_mixer=shape((db, here), F32),
        out_gate=shape((width, hidden), F32),
        out_up=shape((width, hidden), F32),
        out_down=shape((hidden, width), F32),
    )
    scratch = {"v_" + name: pltpu.VMEM(inputs[name].shape, inputs[name].dtype) for name in INPUTS}
    scratch |= dict(
        first=pltpu.VMEM((slots, tokens), BF16),
        second=pltpu.VMEM((slots, tokens), BF16),
        places=pltpu.VMEM((tokens, slots), BF16),
        send_rows=pltpu.VMEM((slots - near * pcap, column), BF16),
        send_cots=pltpu.VMEM((slots - near * pcap, column), BF16),
        near_rows=pltpu.VMEM(((near - 1) * pcap, half * column), BF16),
        near_cots=pltpu.VMEM(((near - 1) * pcap, half * column), BF16),
        rows=pltpu.VMEM((slots, width), BF16),
        cots=pltpu.VMEM((slots, width), BF16),
        hidden=pltpu.VMEM((slots, hidden), BF16),
        back_w=pltpu.VMEM((2 * hidden, width), BF16),
        down_t=pltpu.VMEM((width, hidden), BF16),
        gpg=pltpu.VMEM((slots, hidden), BF16),
        gpu=pltpu.VMEM((slots, hidden), BF16),
        partial=pltpu.VMEM((slots, width), BF16),
        halves=pltpu.VMEM((slots, half * column), BF16),
        passing=pltpu.VMEM((slots, half * column), BF16),
        crossed=pltpu.VMEM((slots, max(1, half - 1) * column), BF16),
        outgoing=pltpu.VMEM((slots, column), BF16),
        back=pltpu.VMEM((slots, column), BF16),
        grad_normed=pltpu.VMEM((tokens, width), BF16),
        grad_stream=pltpu.VMEM((tokens, width), BF16),
        staged=pltpu.VMEM(staged, BF16),
        grad_all=pltpu.VMEM((n * tokens, pdb), BF16),
        act_all=pltpu.VMEM((n * tokens, here), BF16),
        stats=pltpu.VMEM((groups, 8, tokens), F32),
        slopes=pltpu.VMEM((groups, 8, tokens), F32),
        halo_out=pltpu.VMEM((hpad, here), BF16),
        halo_in=pltpu.VMEM((hpad, here), BF16),
        ext=pltpu.VMEM((tokens + hpad, here), F32),
        load=dma((len(INPUTS),)),
    )
    for name, dims in dict(
        sp=(2, n),
        near=(2, near, half),
        share=(2, near, half),
        tp=(2, n, groups),
        st=(groups,),
        core=(chunks, half),
        x=(chunks, half),
        home=(n,),
        gn=(groups,),
        act=(n,),
        gs=(n,),
        ga=(n, groups),
        sl=(groups,),
        halo=(),
    ).items():
        scratch[name + "_send"] = dma(dims)
        scratch[name + "_recv"] = dma(dims)
    names = (*INPUTS, *OUTPUTS, *scratch)
    vmem, hbm = pltpu.VMEM, pltpu.HBM
    results = pl.pallas_call(
        functools.partial(layer_kernel, n, groups, pcap, names),
        out_shape=[pltpu.VMEM(outs[name].shape, outs[name].dtype) for name in OUTPUTS],
        in_specs=[pl.BlockSpec(memory_space=hbm)] * len(INPUTS),
        out_specs=[pl.BlockSpec(memory_space=vmem)] * len(OUTPUTS),
        scratch_shapes=list(scratch.values()),
        compiler_params=pltpu.CompilerParams(
            collective_id=0, has_side_effects=True, vmem_limit_bytes=54 << 20
        ),
    )(*(inputs[name] for name in INPUTS))
    results = pl.pallas_call(
        flush_kernel,
        out_shape=[outs[name] for name in OUTPUTS],
        in_specs=[pl.BlockSpec(memory_space=vmem)] * len(OUTPUTS),
        out_specs=[pl.BlockSpec(memory_space=hbm)] * len(OUTPUTS),
        scratch_shapes=[dma((len(OUTPUTS),))],
        compiler_params=pltpu.CompilerParams(vmem_limit_bytes=1 << 20),
    )(*results)
    value, gating, mixer, gate, up, down = results
    return value, gating, mixer, gate[None], up[None], down[None]


def solution(mesh):
    return jax.shard_map(
        body,
        mesh=mesh,
        in_specs=(
            P("sp", None),
            P("sp", None),
            P(),
            P("sp", None),
            P("sp"),
            P("sp", None),
            P("sp", None, "tp"),
            P("sp", None, "tp"),
            P("sp", "tp", None),
            P("tp", None),
            P("sp", "tp"),
            P("tp"),
            P(None, "tp"),
            P("sp", "tp"),
            P("sp", "tp"),
        ),
        out_specs=(
            P("sp", "tp"),
            P("sp", "tp"),
            P("sp", "tp"),
            P("sp", None, "tp"),
            P("sp", None, "tp"),
            P("sp", "tp", None),
        ),
        check_vma=False,
    )
```

time: 112 us -> 79.6 us (0.71)
  Pallas kernels: 91.4 us -> 78.4 us
  matrix products: 10 us -> 0 us
  local copies, waits for them, and re-layouts: 9.75 us -> 0 us
    pallas_call x2, Pallas kernels: 91.4 us -> 78.4 us  [the longest x1 75.5 us: body(): pl.pallas_call(functools.partial(layer_kernel, n, groups, pcap, names), o...]
    dot_general x8 -> x0, matrix products: 10 us -> none  [the longest x3 6.22 us: contract_first(): lax.dot_general(left, right, (((0,), (0,)), ((), ())), preferred_element_...]
    unnamed x30 -> x0, local copies, waits for them, and re-layouts: 8.1 us -> none
where the time goes in v1:
time: 79.6 us; the launch traced here: 79.2 us
  Pallas kernels  78.4 us (98%)
  between operations  0.81 us (1%)
    pallas_call x1, Pallas kernels, body(): pl.pallas_call(functools.partial(layer_kernel, n, groups, pcap, names), o...  75.5 us
    pallas_call x1, Pallas kernels, body(): pl.pallas_call(flush_kernel, out_shape=[outs[name] for name in OUTPUTS],...  2.91 us

profile of v1, /device:TPU:0, one launch (start us, length us, event | category | flops | bytes accessed | tf_op | source)
XLA Modules:
  0.0 79.2 jit_solution(3829813979959481116)
XLA Ops:
  0.6 75.5 %shard_map.190 = (bf16[192,256]{1,0:T(8,128)(2,1)S(1)}, bf16[192,256]{1,0:T(8,128)(2,1)S(1)}, f32[256,256]{1,0:T(8,128)S(1)}, f32[2048,256]{1,0:T(8,128)S(1)}, f...) custom-call(s32[2,192]{1,0:T(2,128)} %bitcast.15, f32[1,192]{1,0:T(1,128)} %bitcast.17, f32[2,192]{1,0:T(2,128)} %bitcast.16, ...), custom_call_target="tpu_custom_call" | custom-call | tf_op jit(solution)/shard_map/pallas_call | solution.py:973
  76.1 2.9 %shard_map.191 = (bf16[192,256]{1,0:T(8,128)(2,1)}, bf16[192,256]{1,0:T(8,128)(2,1)}, f32[256,256]{1,0:T(8,128)}, f32[2048,256]{1,0:T(8,128)}, f32[2048,256]{1,0:T(8,128)}, /*index=5*/f32[256,2048]{1,0:T(8,128)}) custom-call(bf16[192,256]{1,0:T(8,128)(2,1)S(1)} %get-tuple-element.18.refs_0_, bf16[192,256]{1,0:T(8,128)(2,1)S(1)} %get-tuple-element.19.refs_1_, ...), custom_call_target="tpu_custom_call" | custom-call | tf_op jit(solution)/shard_map/pallas_call | solution.py:983

commit v2 on v1

--- a/solution.py
+++ b/solution.py
@@ -80,24 +80,23 @@
 
 
 class Spread:
-    def __init__(self, axis, place, index, count, send, recv):
+    def __init__(self, axis, place, index, count, send, recv, last):
         self.axis, self.place, self.index, self.count = axis, place, index, count
-        self.send_sem, self.recv_sem = send, recv
+        self.send_sem, self.recv, self.last = send, recv, last
+
+    def recv_sem(self, mask):
+        return self.last if mask % 2 else self.recv(mask // 2 - 1)
 
     def copy(self, mask, bit):
         ref = self.place(flip(self.index, mask))
         return remote(
-            ref,
-            ref,
-            self.send_sem(mask | bit),
-            self.recv_sem(mask | bit),
-            {self.axis: flip(self.index, bit)},
+            ref, ref, self.send_sem, self.recv_sem(mask | bit), {self.axis: flip(self.index, bit)}
         )
 
     def wait(self, mask):
         ref = self.place(flip(self.index, mask))
         where = {self.axis: flip(self.index, low_bit(mask))}
-        remote(ref, ref, self.send_sem(mask), self.recv_sem(mask), where).wait_recv()
+        remote(ref, ref, self.send_sem, self.recv_sem(mask), where).wait_recv()
 
     def begin(self):
         for bit in bits_below(self.count):
@@ -114,42 +113,36 @@
                 for bit in onward:
                     self.copy(mask, bit).start()
 
-    def arrived(self):
-        for mask in self.masks():
-            if not bits_below(low_bit(mask)):
-                self.wait(mask)
-
-    def sent(self):
-        for mask in range(1, self.count):
-            self.copy(mask - low_bit(mask), low_bit(mask)).wait_send()
+    def arrived(self, ref):
+        where = {self.axis: flip(self.index, 1)}
+        remote(ref, ref, self.send_sem, self.last, where).wait_recv()
+
+    def sent(self, ref):
+        where = {self.axis: flip(self.index, 1)}
+        remote(ref, ref, self.send_sem, self.last, where).wait_send()
 
 
 class Direct:
-    def __init__(self, place, index, count, send, recv):
+    def __init__(self, place, index, count, send, recv, others):
         self.place, self.index, self.count = place, index, count
-        self.send_sem, self.recv_sem = send, recv
-
-    def copy(self, mask, origin):
-        ref = self.place(origin)
-        return remote(
-            ref, ref, self.send_sem.at[mask], self.recv_sem.at[mask], {"tp": flip(self.index, mask)}
-        )
+        self.send_sem, self.recv_sem, self.others = send, recv, others
+
+    def copy(self, ref, mask):
+        return remote(ref, ref, self.send_sem, self.recv_sem, {"tp": flip(self.index, mask)})
 
     def begin(self):
         for mask in range(1, self.count):
-            self.copy(mask, self.index).start()
+            self.copy(self.place(self.index), mask).start()
 
     def arrived(self):
-        for mask in range(1, self.count):
-            self.copy(mask, flip(self.index, mask)).wait_recv()
+        self.copy(self.others, 1).wait_recv()
 
     def sent(self):
-        for mask in range(1, self.count):
-            self.copy(mask, self.index).wait_send()
+        self.copy(self.others, 1).wait_send()
 
 
 def bands_of(n):
-    sizes = (n // 4, n // 4, n // 4, n // 8, n // 8)
+    sizes = (n // 4, n // 4, n // 8, n // 8, n // 8, n // 8)
     found, first = [], 0
     for size in sizes:
         found.append((first, first + size))
@@ -328,15 +321,15 @@
         return remote(
             close[a].at[block(m - 1), pl.ds(h * column, column)],
             pairs[a][1].at[block(m), lane_q(h)],
-            r["near_send"].at[a, m, h],
-            r["near_recv"].at[a, m, h],
+            r["near_send"].at[a],
+            r["near_recv"].at[a, m],
             {"sp": peer(m)},
         )
 
     def core_share(a, m, h):
         ref = pairs[a][1].at[block(m), lane_q(h)]
         return remote(
-            ref, ref, r["share_send"].at[a, m, h], r["share_recv"].at[a, m, h], {"tp": flip(tp, 1)}
+            ref, ref, r["share_send"].at[a], r["share_recv"].at[m], {"tp": flip(tp, 1)}
         )
 
     def sp_copy(a, m):
@@ -344,8 +337,8 @@
         return remote(
             src.at[block(m - near)],
             full.at[block(m), mine_q],
-            r["sp_send"].at[a, m],
-            r["sp_recv"].at[a, m],
+            r["sp_send"].at[a],
+            r["sp_recv"].at[a, m - near],
             {"sp": peer(m)},
         )
 
@@ -365,12 +358,12 @@
         each(lo, min(hi, near), send_near)
         each(max(lo, near), hi, send)
 
-    parts = ((1, n // 4), (n // 2, 3 * n // 4), (n // 4, n // 2), (3 * n // 4, n))
-    send_any(*parts[0])
+    send_any(1, n // 4)
     with scope("rows2"):
         stage(mine_q, near, n, slice(0, (n - near) * pcap), r["send_rows"], r["send_cots"])
-    for lo, hi in parts[1:]:
-        send_any(lo, hi)
+    send_any(n // 2, 3 * n // 4)
+    send_any(n // 4, n // 2)
+    send_any(3 * n // 4, n)
 
     with scope("stats"):
         load("filtered").wait()
@@ -382,7 +375,14 @@
         total = contract_last(ones, filt)
         total_square = contract_last(ones, high) + contract_last(ones, low)
         r["stats"][tp] = jnp.where(line == 0, total, total_square)
-        sums = Direct(lambda o: r["stats"].at[o], tp, groups, r["st_send"], r["st_recv"])
+        sums = Direct(
+            lambda o: r["stats"].at[o],
+            tp,
+            groups,
+            r["st_send"],
+            r["st_recv"],
+            r["stats"].at[pl.ds(0, groups - 1)],
+        )
         sums.begin()
 
     with scope("own"):
@@ -402,20 +402,25 @@
             lambda o: pairs[a][1].at[block(m), quarter(o)],
             tp,
             groups,
-            lambda k: r["tp_send"].at[a, m, k],
-            lambda k: r["tp_recv"].at[a, m, k],
+            r["tp_send"].at[a],
+            lambda k: r["tp_recv"].at[a, m - near, k],
+            r["tp_last"].at[m - near],
         )
 
     def arrive_near(m):
         for a in range(2):
+            ref = pairs[a][1].at[block(m), pl.ds(0, half * column)]
+            remote(
+                ref, ref, r["near_send"].at[a], r["near_recv"].at[a, m], {"sp": peer(m)}
+            ).wait_recv()
             for h in range(half):
-                near_copy(a, m, h).wait_recv()
                 core_share(a, m, h).start()
 
     def arrived_near(m):
-        for a in range(2):
-            for h in range(half):
-                core_share(a, m, h).wait_recv()
+        ref = r["rows"].at[block(m)]
+        remote(
+            ref, ref, r["share_send"].at[0], r["share_recv"].at[m], {"tp": flip(tp, 1)}
+        ).wait_recv()
 
     def arrive(m):
         for a in range(2):
@@ -427,8 +432,7 @@
             gather(a, m).relay()
 
     def arrived(m):
-        for a in range(2):
-            gather(a, m).arrived()
+        gather(0, m).arrived(r["rows"].at[block(m)])
 
     def band(c):
         return pl.ds(bands[c][0] * pcap, (bands[c][1] - bands[c][0]) * pcap)
@@ -443,6 +447,7 @@
             for k, name in enumerate(("gate_w", "up_w")):
                 r["back_w"][k * turned : (k + 1) * turned, at] = v[name][at].T
             r["down_t"][at] = v["down_w"][:, at].T
+            r["mixer_t"][at] = v["mixer"][:, at].T
 
     def compute(c):
         at = band(c)
@@ -469,8 +474,8 @@
         return remote(
             r["partial"].at[band(c), quarter(lax.rem(mate, 2) + 2 * h)],
             r["halves"].at[band(c), pl.ds(h * column, column)],
-            r["core_send"].at[c, h],
-            r["core_recv"].at[c, h],
+            r["core_send"],
+            r["core_recv"].at[c],
             {"tp": mate},
         )
 
@@ -478,8 +483,8 @@
         return remote(
             r["passing"].at[band(c), quarter(flip(mine, k))],
             r["crossed"].at[band(c), pl.ds((k - 1) * column, column)],
-            r["x_send"].at[c, k],
-            r["x_recv"].at[c, k],
+            r["x_send"],
+            r["x_recv"].at[c, k - 1],
             {"tp": flip(tp, 2 * k)},
         )
 
@@ -487,35 +492,47 @@
         for h in range(half):
             core_copy(c, h).start()
 
-    def add_core(c):
-        for h in range(half):
-            core_copy(c, h).wait_recv()
+    def add_core(c, cross_now=True):
+        ref = r["halves"].at[band(c)]
+        remote(ref, ref, r["core_send"], r["core_recv"].at[c], {"tp": mate}).wait_recv()
         for h in range(half):
             cols = pl.ds(h * column, column)
             own = r["partial"][band(c), quarter(lax.rem(tp, 2) + 2 * h)].astype(F32)
             r["passing"][band(c), cols] = (
                 own + r["halves"][band(c), cols].astype(F32)
             ).astype(BF16)
+        if cross_now:
+            start_cross(c)
+
+    def start_cross(c):
         for k in range(1, half):
             cross(c, k).start()
 
-    def home_copy(m):
+    span = column // 2
+
+    def strip(t):
+        return pl.ds(t * span, span)
+
+    def home_copy(m, t):
         return remote(
-            r["outgoing"].at[block(m)],
-            r["back"].at[block(m)],
-            r["home_send"].at[m],
-            r["home_recv"].at[m],
+            r["outgoing"].at[block(m), strip(t)],
+            r["back"].at[block(m), strip(t)],
+            r["home_send"],
+            r["home_recv"].at[t],
             {"sp": peer(m)},
         )
 
     def add_cross(c):
         for k in range(1, half):
             cross(c, k).wait_recv()
-        total = r["passing"][band(c), quarter(mine)].astype(F32)
-        for k in range(1, half):
-            total = total + r["crossed"][band(c), pl.ds((k - 1) * column, column)].astype(F32)
-        r["outgoing"][band(c)] = total.astype(BF16)
-        each(max(1, bands[c][0]), bands[c][1], lambda m: home_copy(m).start())
+        for t in range(2):
+            at = pl.ds(start_of(2 * mine + t, span), span)
+            total = r["passing"][band(c), at].astype(F32)
+            for k in range(1, half):
+                other = pl.ds((k - 1) * column + t * span, span)
+                total = total + r["crossed"][band(c), other].astype(F32)
+            r["outgoing"][band(c), strip(t)] = total.astype(BF16)
+            each(max(1, bands[c][0]), bands[c][1], lambda m: home_copy(m, t).start())
 
     def act_rows(s):
         return pl.ds(start_of(s, tokens), tokens)
@@ -525,24 +542,26 @@
         lambda o: r["act_all"].at[act_rows(o)],
         me,
         n,
-        lambda m: r["act_send"].at[m],
-        lambda m: r["act_recv"].at[m],
+        r["act_send"],
+        lambda k: r["act_recv"].at[k],
+        r["act_last"],
     )
 
     def early(bit):
         acts.copy(0, bit).start()
 
-    def arrivals(lo, hi):
+    def arrivals(lo, hi, base=None):
+        base = max(lo if base is None else base, near)
         with scope("arrive#m=%d" % lo):
             each(lo, min(hi, near), arrive_near)
 
             def step(m):
                 arrive(m)
                 if isinstance(m, int):
-                    if m > max(lo, near):
+                    if m > base:
                         relay(m - 1)
                 else:
-                    pl.when(m > max(lo, near))(lambda: relay(m - 1))
+                    pl.when(m > base)(lambda: relay(m - 1))
 
             each(max(lo, near), hi, step)
 
@@ -561,9 +580,39 @@
             start_core(c)
 
     with scope("turn"):
-        for name in ("gate_w", "up_w", "down_w"):
+        for name in ("gate_w", "up_w", "down_w", "mixer"):
             load(name).wait()
         turn()
+    def addcore(c, cross_now=True):
+        with scope("addcore#c=%d" % c):
+            add_core(c, cross_now)
+
+    def addcross(c):
+        with scope("addcross#c=%d" % c):
+            add_cross(c)
+
+    def act_relay(masks):
+        for mask in masks:
+            onward = bits_below(low_bit(mask))
+            if onward:
+                acts.wait(mask)
+                for bit in onward:
+                    acts.copy(mask, bit).start()
+
+    act_masks = acts.masks()
+    last = len(bands) - 1
+    one, two, mid, three, final = (bands[c][0] for c in range(1, 6))
+    arrivals(1, one)
+    lastrelay(one)
+    whole(0)
+    arrivals(two, mid)
+    arrivals(mid, three, mid)
+    addcore(0)
+    lastrelay(mid)
+    whole(2)
+    lastrelay(three)
+    addcore(2)
+    whole(3)
     with scope("normact"):
         sums.arrived()
         moments = r["stats"][0]
@@ -583,61 +632,37 @@
         _, normal_out, sig_norm = norms()
         r["act_all"][act_rows(me)] = (normal_out * sig_norm).astype(BF16)
 
-    def addcore(c):
-        with scope("addcore#c=%d" % c):
-            add_core(c)
-
-    def addcross(c):
-        with scope("addcross#c=%d" % c):
-            add_cross(c)
-
-    def act_relay(masks):
-        for mask in masks:
-            onward = bits_below(low_bit(mask))
-            if onward:
-                acts.wait(mask)
-                for bit in onward:
-                    acts.copy(mask, bit).start()
-
-    act_masks = acts.masks()
-    quarter_n, last = n // 4, len(bands) - 1
-    one, two, three = bands[1][0], bands[2][0], bands[3][0]
-    final = bands[4][0]
-    arrivals(1, one)
-    lastrelay(one)
-    whole(0)
-    arrivals(two, three)
-    addcore(0)
-    lastrelay(three)
-    whole(2)
+    addcore(3)
     addcross(0)
     arrivals(one, two)
-    addcore(2)
     lastrelay(two)
+    arrivals(three, final)
     whole(1)
-    arrivals(three, final)
+    arrivals(final, n)
+    addcross(2)
     addcore(1)
-    addcross(2)
-    arrivals(final, n)
-    lastrelay(final)
-    whole(3)
+    addcross(3)
     for bit in bits_below(n):
         early(bit)
+    lastrelay(final)
+    whole(4)
     lastrelay(n)
+    addcore(4)
+    whole(5)
     addcross(1)
-    addcore(3)
-    whole(4)
-    addcross(3)
-    addcore(4)
+    addcore(5)
+    addcross(4)
+    with scope("actrelay1"):
+        act_relay([m for m in act_masks if m < top])
 
     tile = min(256, width)
 
-    def wgrad(left, pick):
+    def wgrad(left, pick, lo=0, hi=width // tile):
         def step(t):
             cols = pl.ds(start_of(t, tile), tile)
             r[pick][cols] = contract_first(r["rows"][:, cols], r[left][...])
 
-        lax.fori_loop(0, width // tile, lambda t, c: (step(t), c)[1], 0)
+        lax.fori_loop(lo, hi, lambda t, c: (step(t), c)[1], 0)
 
     def wgrad_down():
         def step(t):
@@ -647,34 +672,50 @@
         lax.fori_loop(0, width // tile, lambda t, c: (step(t), c)[1], 0)
 
     with scope("wgrad_gate"):
-        wgrad("gpg", "out_gate")
+        wgrad("gpg", "out_gate", 0, width // tile * 7 // 8)
     with scope("addcross#c=%d" % last):
         add_cross(last)
         r["back"][0:pcap] = r["outgoing"][0:pcap]
+    with scope("actrelay2"):
+        act_relay([top])
     with scope("wgrad_up"):
+        wgrad("gpg", "out_gate", width // tile * 7 // 8, width // tile)
         wgrad("gpu", "out_up")
-    with scope("home"):
-        each(1, n, lambda m: home_copy(m).wait_recv())
-    with scope("combine"):
-        r["grad_normed"][:, mine_q] = dot(r["places"][...], r["back"][...]).astype(BF16)
-        normal = Spread(
+    with scope("norms"):
+        centred, normal_out, sig_norm = norms()
+        r["centred"][...] = centred
+        r["bend"][...] = silu_slope(normal_out, sig_norm) * v["channel_gain"][...]
+    def homes(t):
+        ref = r["back"].at[pl.ds(pcap, slots - pcap), strip(t)]
+        return remote(ref, ref, r["home_send"], r["home_recv"].at[t], {"sp": peer(1)})
+
+    def normal(t):
+        return Spread(
             "tp",
-            lambda o: r["grad_normed"].at[:, quarter(o)],
+            lambda o: r["grad_normed"].at[:, pl.ds(start_of(2 * o + t, span), span)],
             tp,
             groups,
-            lambda m: r["gn_send"].at[m],
-            lambda m: r["gn_recv"].at[m],
-        )
-        normal.begin()
-    with scope("actrelay2"):
-        act_relay([m for m in act_masks if m <= top])
+            r["gn_send"],
+            lambda k: r["gn_recv"].at[t, k],
+            r["gn_last"],
+        )
+
+    for t in range(2):
+        with scope("home#t=%d" % t):
+            homes(t).wait_recv()
+        with scope("combine#t=%d" % t):
+            r["grad_normed"][:, pl.ds(start_of(2 * tp + t, span), span)] = dot(
+                r["places"][...], r["back"][:, strip(t)]
+            ).astype(BF16)
+            normal(t).begin()
     with scope("wgrad_down"):
         wgrad_down()
     with scope("actrelay3"):
         act_relay([m for m in act_masks if m > top])
     with scope("gather"):
-        normal.relay()
-        normal.arrived()
+        for t in range(2):
+            normal(t).relay()
+        normal(0).arrived(r["grad_normed"].at[:, pl.ds(0, half * column)])
 
     with scope("gradstream"):
         inner = jnp.zeros((tokens, 1), F32)
@@ -698,15 +739,21 @@
         start = pl.multiple_of(s * tokens + o * portion, portion)
         return r["grad_all"].at[pl.ds(start, portion)]
 
-    my_rows = pl.ds(pl.multiple_of(tp * portion, portion), portion)
+    def parts_of(count):
+        return r["grad_all"].at[pl.ds(0, count * portion)]
+
+    def rows_of(h):
+        return pl.ds(pl.multiple_of((side + 2 * h) * portion, portion), portion)
+
     if db == pdb:
 
-        def cut(j):
-            return r["grad_stream"].at[my_rows, pl.ds(pl.multiple_of(j * db, db), db)]
-
-        r["grad_all"][act_rows(me)] = r["grad_stream"][
-            :, pl.ds(pl.multiple_of(me * db, db), db)
-        ]
+        def cut(j, h):
+            return r["grad_stream"].at[rows_of(h), pl.ds(pl.multiple_of(j * db, db), db)]
+
+        def own_cut():
+            r["grad_all"][act_rows(me)] = r["grad_stream"][
+                :, pl.ds(pl.multiple_of(me * db, db), db)
+            ]
     else:
 
         def pick(j):
@@ -714,18 +761,28 @@
             lane = lax.broadcasted_iota(jnp.int32, (width, pdb), 1)
             return ((where == lane + j * db) & (lane < db)).astype(F32).astype(BF16)
 
-        def stage(j):
-            r["staged"][j] = dot(r["grad_stream"][my_rows], pick(j)).astype(BF16)
-
-        each(0, n, stage)
-
-        def cut(j):
-            return r["staged"].at[j]
-
-        r["grad_all"][act_rows(me)] = dot(r["grad_stream"][...], pick(me)).astype(BF16)
-
-    def cut_copy(m, j, s):
-        return remote(cut(j), part(s, tp), r["gs_send"].at[m], r["gs_recv"].at[m], {"sp": j})
+        def stage_cut(j):
+            for h in range(half):
+                r["staged"][j, h * portion : (h + 1) * portion] = dot(
+                    r["grad_stream"][rows_of(h)], pick(j)
+                ).astype(BF16)
+
+        each(0, n, stage_cut)
+
+        def cut(j, h):
+            return r["staged"].at[j, pl.ds(start_of(h, portion), portion)]
+
+        def own_cut():
+            r["grad_all"][act_rows(me)] = dot(r["grad_stream"][...], pick(me)).astype(BF16)
+
+    def cut_copy(m, h, j, s):
+        return remote(
+            cut(j, h), part(s, side + 2 * h), r["gs_send"], r["gs_recv"].at[m], {"sp": j}
+        )
+
+    def cut_sends_near(m):
+        for h in range(half):
+            cut_copy(m, h, peer(m), me).start()
 
     def spread_cut(m):
         s = peer(m)
@@ -734,30 +791,44 @@
             lambda o: part(s, o),
             tp,
             groups,
-            lambda k: r["ga_send"].at[m, k],
+            r["ga_send"],
             lambda k: r["ga_recv"].at[m, k],
-        )
+            r["ga_last"],
+        )
+
+    def cut_arrives_near(m):
+        ref = parts_of(half)
+        remote(ref, ref, r["gs_send"], r["gs_recv"].at[m], {"sp": peer(m)}).wait_recv()
+        for h in range(half):
+            ref = part(peer(m), side + 2 * h)
+            remote(ref, ref, r["ga_send"], r["ga_last"], {"tp": mate}).start()
 
     def cut_arrives(m):
-        cut_copy(m, peer(m), peer(m)).wait_recv()
+        cut_copy(m, mine, peer(m), peer(m)).wait_recv()
         spread_cut(m).begin()
 
     with scope("cutstart"):
-        each(1, n, lambda m: cut_copy(m, peer(m), me).start())
+        each(near, n, lambda m: cut_copy(m, mine, peer(m), me).start())
+        each(1, near, cut_sends_near)
 
     with scope("slopes"):
-        load("mixer").wait()
-        grad_act = contract_last(r["grad_stream"][...], v["mixer"][...])
-        centred, normal_out, sig_norm = norms()
-        grad_centred = grad_act * silu_slope(normal_out, sig_norm) * v["channel_gain"][...]
+        grad_act = dot(r["grad_stream"][...], r["mixer_t"][...])
+        centred = r["centred"][...]
+        grad_centred = grad_act * r["bend"][...]
         ones = jnp.ones((8, here), F32)
         slope_sum = contract_last(ones, grad_centred, HIGHEST)
         slope_cross = contract_last(ones, grad_centred * centred, HIGHEST)
         r["slopes"][tp] = jnp.where(line == 0, slope_sum, slope_cross)
-        meet = Direct(lambda o: r["slopes"].at[o], tp, groups, r["sl_send"], r["sl_recv"])
+        meet = Direct(
+            lambda o: r["slopes"].at[o],
+            tp,
+            groups,
+            r["sl_send"],
+            r["sl_recv"],
+            r["slopes"].at[pl.ds(0, groups - 1)],
+        )
         meet.begin()
-    with scope("cutarrive1"):
-        each(1, top, cut_arrives)
+        own_cut()
     with scope("meet"):
         meet.arrived()
     with scope("gradfiltered"):
@@ -790,13 +861,13 @@
         ).astype(BF16)
 
     with scope("cutarrive2"):
-        each(top, n - n // 4, cut_arrives)
+        each(near, n, cut_arrives)
+    with scope("cutarrive1"):
+        each(1, near, cut_arrives_near)
     with scope("conv1"):
         for name in ("taps", "value", "gate"):
             load(name).wait()
         conv(0, tokens - hpad)
-    with scope("cutarrive3"):
-        each(n - n // 4, n, cut_arrives)
     with scope("halo"):
         halo_copy().wait_recv()
         inside = jnp.where(me < n - 1, 1.0, 0.0)
@@ -804,45 +875,39 @@
     with scope("conv2"):
         conv(tokens - hpad, tokens)
     with scope("cutrelay"):
-        each(1, n, lambda m: spread_cut(m).relay())
+        each(near, n, lambda m: spread_cut(m).relay())
     with scope("cutwait"):
-        each(1, n, lambda m: spread_cut(m).arrived())
+        spread_cut(1).arrived(parts_of((n - 1) * half))
     with scope("actwait"):
-        acts.arrived()
+        acts.arrived(r["act_all"].at[pl.ds(0, n // 2 * tokens)])
     with scope("mixer"):
         r["out_mixer"][...] = contract_first(r["grad_all"][...], r["act_all"][...])[:db]
 
     with scope("drain"):
 
-        def sent(m):
-            home_copy(m).wait_send()
-            cut_copy(m, peer(m), me).wait_send()
-            spread_cut(m).sent()
-
-        def sent_near(m):
-            for a in range(2):
-                for h in range(half):
-                    near_copy(a, m, h).wait_send()
-                    core_share(a, m, h).wait_send()
-
-        def sent_far(m):
-            for a in range(2):
-                sp_copy(a, m).wait_send()
-                gather(a, m).sent()
-
-        each(1, near, sent_near)
-        each(near, n, sent_far)
-        each(1, n, sent)
+        def gone(ref, sem, where):
+            remote(ref, ref, sem, r["halo_recv"], where).wait_send()
+
+        sp_one, tp_one = {"sp": peer(1)}, {"tp": mate}
+        far_rows = pl.ds(0, (n - near) * pcap)
+        for a in range(2):
+            gone(close[a], r["near_send"].at[a], sp_one)
+            gone(close[a], r["share_send"].at[a], tp_one)
+            gone(pairs[a][0], r["sp_send"].at[a], sp_one)
+            ref = pairs[a][1].at[far_rows, pl.ds(0, (groups - 1) * column)]
+            gone(ref, r["tp_send"].at[a], tp_one)
+        gone(r["halves"], r["core_send"], tp_one)
+        if half > 1:
+            gone(r["crossed"], r["x_send"], tp_one)
+        gone(r["back"].at[pl.ds(pcap, slots - pcap)], r["home_send"], sp_one)
+        close_cuts, far_cuts = (near - 1) * half, n - near
+        gone(parts_of(close_cuts + far_cuts), r["gs_send"], sp_one)
+        gone(parts_of(close_cuts + far_cuts * (groups - 1)), r["ga_send"], tp_one)
+        gone(r["act_all"].at[pl.ds(0, (n - 1) * tokens)], r["act_send"], sp_one)
+        gone(r["grad_normed"].at[:, pl.ds(0, (groups - 1) * column)], r["gn_send"], tp_one)
         sums.sent()
-        normal.sent()
         meet.sent()
-        acts.sent()
         halo_copy().wait_send()
-        for c in range(len(bands)):
-            for h in range(half):
-                core_copy(c, h).wait_send()
-            for k in range(1, half):
-                cross(c, k).wait_send()
 
 
 def flush_kernel(*refs):
@@ -886,7 +951,7 @@
     db = width // n
     pdb = round_up(db, 128)
     hpad = round_up(kernel_taps.shape[0] - 1, 16)
-    staged = (n, tokens // groups, pdb) if pdb != db else (1, 16, 128)
+    staged = (n, half * (tokens // groups), pdb) if pdb != db else (1, 16, 128)
     chunks = len(bands_of(n))
     near = direct_of(n)
     dma = pltpu.SemaphoreType.DMA
@@ -930,6 +995,9 @@
         hidden=pltpu.VMEM((slots, hidden), BF16),
         back_w=pltpu.VMEM((2 * hidden, width), BF16),
         down_t=pltpu.VMEM((width, hidden), BF16),
+        mixer_t=pltpu.VMEM((width, here), BF16),
+        centred=pltpu.VMEM((tokens, here), F32),
+        bend=pltpu.VMEM((tokens, here), F32),
         gpg=pltpu.VMEM((slots, hidden), BF16),
         gpu=pltpu.VMEM((slots, hidden), BF16),
         partial=pltpu.VMEM((slots, width), BF16),
@@ -950,24 +1018,42 @@
         ext=pltpu.VMEM((tokens + hpad, here), F32),
         load=dma((len(INPUTS),)),
     )
+    middle = max(1, half - 1)
     for name, dims in dict(
-        sp=(2, n),
-        near=(2, near, half),
-        share=(2, near, half),
-        tp=(2, n, groups),
-        st=(groups,),
-        core=(chunks, half),
-        x=(chunks, half),
-        home=(n,),
-        gn=(groups,),
-        act=(n,),
-        gs=(n,),
-        ga=(n, groups),
-        sl=(groups,),
-        halo=(),
+        near_send=(2,),
+        near_recv=(2, near),
+        share_send=(2,),
+        share_recv=(near,),
+        sp_send=(2,),
+        sp_recv=(2, n - near),
+        tp_send=(2,),
+        tp_recv=(2, n - near, middle),
+        tp_last=(n - near,),
+        st_send=(),
+        st_recv=(),
+        core_send=(),
+        core_recv=(chunks,),
+        x_send=(),
+        x_recv=(chunks, middle),
+        home_send=(),
+        home_recv=(2,),
+        gn_send=(),
+        gn_recv=(2, middle),
+        gn_last=(),
+        act_send=(),
+        act_recv=(n // 2 - 1,),
+        act_last=(),
+        gs_send=(),
+        gs_recv=(n,),
+        ga_send=(),
+        ga_recv=(n, middle),
+        ga_last=(),
+        sl_send=(),
+        sl_recv=(),
+        halo_send=(),
+        halo_recv=(),
     ).items():
-        scratch[name + "_send"] = dma(dims)
-        scratch[name + "_recv"] = dma(dims)
+        scratch[name] = dma(dims)
     names = (*INPUTS, *OUTPUTS, *scratch)
     vmem, hbm = pltpu.VMEM, pltpu.HBM
     results = pl.pallas_call(

time: 79.6 us -> 72 us (0.905)
  Pallas kernels: 78.4 us -> 71 us
    pallas_call x1, Pallas kernels: 75.5 us -> 68.1 us  [body(): pl.pallas_call(functools.partial(layer_kernel, n, groups, pcap, names), o...]
where the time goes in v2:
time: 72 us; the launch traced here: 71.8 us
  Pallas kernels  71 us (99%)
  between operations  0.81 us (1%)
    pallas_call x1, Pallas kernels, body(): pl.pallas_call(functools.partial(layer_kernel, n, groups, pcap, names), o...  68.1 us
    pallas_call x1, Pallas kernels, body(): pl.pallas_call(flush_kernel, out_shape=[outs[name] for name in OUTPUTS],...  2.91 us

profile of v2, /device:TPU:0, one launch (start us, length us, event | category | flops | bytes accessed | tf_op | source)
XLA Modules:
  0.0 71.8 jit_solution(4881874283421542586)
XLA Ops:
  0.6 68.1 %shard_map.190 = (bf16[192,256]{1,0:T(8,128)(2,1)S(1)}, bf16[192,256]{1,0:T(8,128)(2,1)S(1)}, f32[256,256]{1,0:T(8,128)S(1)}, f32[2048,256]{1,0:T(8,128)S(1)}, f...) custom-call(s32[2,192]{1,0:T(2,128)} %bitcast.15, f32[1,192]{1,0:T(1,128)} %bitcast.17, f32[2,192]{1,0:T(2,128)} %bitcast.16, ...), custom_call_target="tpu_custom_call" | custom-call | tf_op jit(solution)/shard_map/pallas_call | solution.py:1059
  68.7 2.9 %shard_map.191 = (bf16[192,256]{1,0:T(8,128)(2,1)}, bf16[192,256]{1,0:T(8,128)(2,1)}, f32[256,256]{1,0:T(8,128)}, f32[2048,256]{1,0:T(8,128)}, f32[2048,256]{1,0:T(8,128)}, /*index=5*/f32[256,2048]{1,0:T(8,128)}) custom-call(bf16[192,256]{1,0:T(8,128)(2,1)S(1)} %get-tuple-element.18.refs_0_, bf16[192,256]{1,0:T(8,128)(2,1)S(1)} %get-tuple-element.19.refs_1_, ...), custom_call_target="tpu_custom_call" | custom-call | tf_op jit(solution)/shard_map/pallas_call | solution.py:1069

commit v3 on v2

--- a/solution.py
+++ b/solution.py
@@ -634,9 +634,9 @@
 
     addcore(3)
     addcross(0)
+    arrivals(three, final)
     arrivals(one, two)
     lastrelay(two)
-    arrivals(three, final)
     whole(1)
     arrivals(final, n)
     addcross(2)
@@ -862,12 +862,12 @@
 
     with scope("cutarrive2"):
         each(near, n, cut_arrives)
-    with scope("cutarrive1"):
-        each(1, near, cut_arrives_near)
     with scope("conv1"):
         for name in ("taps", "value", "gate"):
             load(name).wait()
         conv(0, tokens - hpad)
+    with scope("cutarrive1"):
+        each(1, near, cut_arrives_near)
     with scope("halo"):
         halo_copy().wait_recv()
         inside = jnp.where(me < n - 1, 1.0, 0.0)

time: 72 us -> 71.4 us (level)
  no operation moved by 1% of the time
where the time goes in v3:
time: 71.4 us; the launch traced here: 71.2 us
  Pallas kernels  70.4 us (99%)
  between operations  0.81 us (1%)
    pallas_call x1, Pallas kernels, body(): pl.pallas_call(functools.partial(layer_kernel, n, groups, pcap, names), o...  67.5 us
    pallas_call x1, Pallas kernels, body(): pl.pallas_call(flush_kernel, out_shape=[outs[name] for name in OUTPUTS],...  2.91 us

profile of v3, /device:TPU:0, one launch (start us, length us, event | category | flops | bytes accessed | tf_op | source)
XLA Modules:
  0.0 71.2 jit_solution(11236146875423116742)
XLA Ops:
  0.6 67.5 %shard_map.190 = (bf16[192,256]{1,0:T(8,128)(2,1)S(1)}, bf16[192,256]{1,0:T(8,128)(2,1)S(1)}, f32[256,256]{1,0:T(8,128)S(1)}, f32[2048,256]{1,0:T(8,128)S(1)}, f...) custom-call(s32[2,192]{1,0:T(2,128)} %bitcast.15, f32[1,192]{1,0:T(1,128)} %bitcast.17, f32[2,192]{1,0:T(2,128)} %bitcast.16, ...), custom_call_target="tpu_custom_call" | custom-call | tf_op jit(solution)/shard_map/pallas_call | solution.py:1059
  68.2 2.9 %shard_map.191 = (bf16[192,256]{1,0:T(8,128)(2,1)}, bf16[192,256]{1,0:T(8,128)(2,1)}, f32[256,256]{1,0:T(8,128)}, f32[2048,256]{1,0:T(8,128)}, f32[2048,256]{1,0:T(8,128)}, /*index=5*/f32[256,2048]{1,0:T(8,128)}) custom-call(bf16[192,256]{1,0:T(8,128)(2,1)S(1)} %get-tuple-element.18.refs_0_, bf16[192,256]{1,0:T(8,128)(2,1)S(1)} %get-tuple-element.19.refs_1_, ...), custom_call_target="tpu_custom_call" | custom-call | tf_op jit(solution)/shard_map/pallas_call | solution.py:1069
